TPU v7x, 512 devices: a whole 4x8x8 slice. The times are simulated.
512 devices in a mesh: ep: 32 (over z, x), tp: 16 (over y, core).
Axes of the slice: x: 4, y: 8, z: 8, core: 2. Of those that a mesh axis runs over, the one named last changes fastest.
Arguments:
- mix_rows: bfloat16 [8192, 2048], P('ep'), may hold values from -6 to 6
- mix_gain: bfloat16 [2048], replicated, may hold values from 0.099609375 to 1.8984375
- w_query: bfloat16 [1024, 2048], P('tp'), may hold values from -0.125 to 0.125
- w_key: bfloat16 [1024, 2048], P('tp'), may hold values from -0.125 to 0.125
- w_value: bfloat16 [1024, 2048], P('tp'), may hold values from -0.125 to 0.125
- key_offset: float32 [16, 8192], P('tp'), may hold values from -11 to 0
- w_out: bfloat16 [1024, 2048], P('tp'), may hold values from -0.1875 to 0.1875
- out_gain: bfloat16 [2048], replicated, may hold values from 0.099609375 to 1.8984375
- exp_rows: bfloat16 [3072, 2048], P('ep', 'tp'), may hold values from -100 to 100
- exp_gain: bfloat16 [2048], P('tp'), may hold values from 0.099609375 to 1.8984375
- routes: int32 [3072, 4], P('ep'), may hold values from 0 to 31, all different within a row; in each aligned block of 96 rows (0 to 95, 96 to 191, ...) at most 16 rows name the same one
- route_weight: float32 [3072, 4], P('ep'), may hold values from 0.05 to 1
- w_gate: bfloat16 [32, 2048, 2048], P('ep', None, 'tp'), may hold values from -0.5 to 0.5
- w_up: bfloat16 [32, 2048, 2048], P('ep', None, 'tp'), may hold values from -0.5 to 0.5
- w_down: bfloat16 [32, 2048, 2048], P('ep', 'tp'), may hold values from -0.1875 to 0.1875
Outputs:
- mix_out: bfloat16 [8192, 2048], P('ep')
- exp_out: bfloat16 [3072, 2048], P('ep', 'tp')
Inputs may be any that keep to these rules, and one draw needn't show every extreme that they name: `routes`: each row names 4 different experts. Within the rows of one device (aligned blocks of 96 rows) no expert is named by more than 16 rows, and in some blocks one expert is named by exactly 16 rows.
All inputs are finite; a program needn't handle non-finite values.
Results may differ from a plain program's by a relative error of at most 0.019.
Values may be sent and summed in bfloat16 or wider, within the bound.
A program may use at most 128 MiB of HBM per device.

v0:
```python
import math

import jax
import jax.numpy as jnp
from jax import lax
from jax.sharding import Mesh
from jax.sharding import PartitionSpec as P

EP = ("ep_0", "ep_1")
TP = ("tp_0", "tp_1")


EPSILON = 1e-06
CLAMP_LIMIT = 7.0
SILU_SHARPNESS = 1.702


def gathered_by_axis(value, axes, dim):
    out = value
    for number in range(len(axes) - 1, -1, -1):
        out = lax.all_gather(out, axes[number], axis=dim, tiled=True)
    return out


def split_up(value, dim, devices):
    dims = value.shape
    tiles = value.reshape(*dims[:dim], devices, dims[dim] // devices, *dims[dim + 1 :])
    return jnp.moveaxis(tiles, dim, 0)


def sent_and_summed(value, axis, dim):
    devices = lax.axis_size(axis)
    tiles = lax.all_to_all(split_up(value, dim, devices), axis, 0, 0, tiled=True)
    return jnp.sum(tiles.astype(jnp.float32), axis=0)


def from_everyone(value, axis):
    copies = jnp.broadcast_to(value, (lax.axis_size(axis), *value.shape))
    return lax.all_to_all(copies, axis, split_axis=0, concat_axis=0, tiled=True)


def of_everyone(value, axis):
    return from_everyone(value, axis).sum(axis=0)


def gather_turned(arrays, axis, dims):
    turned = [jnp.moveaxis(a, dim, 0) for a, dim in zip(arrays, dims)]
    widths = [t[0].size for t in turned]
    both = jnp.concatenate([t.reshape(-1, w) for t, w in zip(turned, widths)], axis=1)
    out = lax.all_gather(both, axis, axis=0, tiled=True)
    tiles = jnp.split(out, [sum(widths[:k]) for k in range(1, len(widths))], axis=1)
    return tuple(
        (
            jnp.moveaxis(b.reshape(-1, *t.shape[1:]), 0, dim)
            for b, t, dim in zip(tiles, turned, dims)
        )
    )


def summed_rows_2(value, chips, core, dim):
    sizes = (lax.axis_size(chips), lax.axis_size(core))
    tiles = split_up(value, dim, sizes[0] * sizes[1])
    inside = tiles.shape[1:]
    tiles = tiles.reshape(*sizes, *inside).swapaxes(0, 1).reshape(-1, *inside)
    tiles = lax.psum_scatter(tiles, core, scatter_dimension=0, tiled=True)
    return lax.psum_scatter(tiles, chips, scatter_dimension=0, tiled=True)[0]


def normalize(numbers, gain):
    factor = lax.rsqrt(jnp.mean(numbers * numbers, axis=-1, keepdims=True) + EPSILON)
    return numbers * factor * gain.astype(jnp.float32)


def project(normed, weight):
    product = lax.dot_general(
        normed, weight, (((1,), (1,)), ((), ())), preferred_element_type=jnp.float32
    )
    return product.astype(jnp.bfloat16)


def gated_units(gate_pre, up_pre):
    gate_part = jnp.minimum(gate_pre, CLAMP_LIMIT)
    up_part = jnp.clip(up_pre, -CLAMP_LIMIT, CLAMP_LIMIT)
    return (up_part + 1.0) * (gate_part * jax.nn.sigmoid(SILU_SHARPNESS * gate_part))


def stick_terms(queries, block_pairs, offset_values, query_index, key_index):
    heads_here = queries.shape[1]
    head_size = queries.shape[2]
    width = heads_here * head_size
    key_rows = block_pairs[:, :width].reshape(-1, heads_here, head_size)
    value_rows = block_pairs[:, width:].reshape(-1, heads_here, head_size)
    scores = jnp.einsum(
        "thd,shd->hts", queries, key_rows, preferred_element_type=jnp.float32
    ) / math.sqrt(head_size)
    scores = scores + offset_values[:, None, :]
    visible = (key_index[None, :] < query_index[:, None])[None]
    keep_log = jnp.where(visible, jax.nn.log_sigmoid(-scores), 0.0)
    later_sum = lax.cumsum(keep_log, axis=2, reverse=True) - keep_log
    exponent = jax.nn.log_sigmoid(scores) + later_sum
    weights = jnp.where(visible, jnp.exp(exponent), 0.0).astype(jnp.bfloat16)
    attended = jnp.einsum("hts,shd->thd", weights, value_rows, preferred_element_type=jnp.float32)
    return (attended, jnp.sum(keep_log, axis=2))


def on_device(
    mix_rows,
    mix_gain,
    w_query,
    w_key,
    w_value,
    key_offset,
    w_out,
    out_gain,
    exp_rows,
    exp_gain,
    routes,
    route_weight,
    w_gate,
    w_up,
    w_down,
):
    row_count = mix_rows.shape[0]
    heads_here = key_offset.shape[0]
    head_size = w_query.shape[0] // heads_here
    normed = normalize(mix_rows.astype(jnp.float32), mix_gain).astype(jnp.bfloat16)
    queries = project(normed, w_query).reshape(row_count, heads_here, head_size)
    own_pairs = jnp.concatenate([project(normed, w_key), project(normed, w_value)], axis=1)
    own_start = lax.axis_index(EP) * row_count
    query_index = own_start + jnp.arange(row_count, dtype=jnp.int32)
    every_pair = gathered_by_axis(own_pairs, EP, 0)
    key_index = jnp.arange(every_pair.shape[0], dtype=jnp.int32)
    attended, _ = stick_terms(queries, every_pair, key_offset, query_index, key_index)
    attended = attended.reshape(row_count, heads_here * head_size).astype(jnp.bfloat16)
    tp_count = lax.axis_size(TP)
    model_width = w_out.shape[1]
    column_count = model_width // tp_count
    columns = w_out
    share = sent_and_summed(
        lax.dot_general(
            columns, attended, (((0,), (1,)), ((), ())), preferred_element_type=jnp.float32
        ).astype(jnp.bfloat16),
        TP,
        0,
    )
    row_sums = of_everyone(jnp.sum(share * share, axis=0), TP)
    factor = lax.rsqrt(row_sums / model_width + EPSILON)
    gain_share = lax.dynamic_slice_in_dim(
        out_gain, lax.axis_index(TP) * column_count, column_count, 0
    ).astype(jnp.float32)
    own_columns = (share.T * factor[:, None] * gain_share[None, :]).astype(jnp.bfloat16)
    mix_out = lax.all_gather(own_columns, TP, axis=1, tiled=True)
    token_count, top_count = routes.shape
    ep_count = lax.axis_size(EP)
    experts = w_gate.shape[0] * ep_count
    capacity = 4 * token_count * top_count // (3 * experts)
    route_list = routes.reshape(-1)
    matches = (route_list[:, None] == jnp.arange(experts, dtype=jnp.int32)[None, :]).astype(
        jnp.int32
    )
    earlier = jnp.cumsum(matches, axis=0) - matches
    slot_index = route_list * capacity + jnp.sum(earlier * matches, axis=1)
    token_of = jnp.arange(route_list.shape[0], dtype=jnp.int32) // top_count + 1
    owners = jnp.zeros((experts * capacity,), jnp.int32).at[slot_index].set(token_of)
    whole_rows, whole_gain = gather_turned((exp_rows, exp_gain), TP, (1, 0))
    normed_exp = normalize(whole_rows.astype(jnp.float32), whole_gain).astype(jnp.bfloat16)
    outgoing = jnp.where(
        owners[:, None] > 0, normed_exp[jnp.maximum(owners - 1, 0)], jnp.zeros((), jnp.bfloat16)
    )
    arrived = lax.all_to_all(outgoing, EP, split_axis=0, concat_axis=0, tiled=True)
    gate_pre = jnp.dot(arrived, w_gate[0], preferred_element_type=jnp.float32)
    up_pre = jnp.dot(arrived, w_up[0], preferred_element_type=jnp.float32)
    hidden = gated_units(gate_pre, up_pre).astype(jnp.bfloat16)
    columns = w_down[0]
    expert_out = (
        summed_rows_2(
            lax.dot_general(
                columns, hidden, (((0,), (1,)), ((), ())), preferred_element_type=jnp.float32
            ).astype(jnp.bfloat16),
            "tp_0",
            "tp_1",
            0,
        )
        .astype(jnp.float32)
        .astype(jnp.bfloat16)
    )
    returned = lax.all_to_all(expert_out, EP, split_axis=1, concat_axis=1, tiled=True)
    picked = (
        jnp.take(returned, slot_index, axis=1)
        .astype(jnp.float32)
        .reshape(-1, token_count, top_count)
    )
    combined = jnp.sum(picked * route_weight[None], axis=2)
    exp_out = combined.T.astype(jnp.bfloat16)
    return (mix_out, exp_out)


def solution(mesh):
    torus = Mesh(mesh.devices.reshape(8, 4, 8, 2), ("ep_0", "ep_1", "tp_0", "tp_1"))
    in_specs = (
        P(EP, None),
        P(),
        P(TP, None),
        P(TP, None),
        P(TP, None),
        P(TP, None),
        P(TP, None),
        P(),
        P(EP, TP),
        P(TP),
        P(EP, None),
        P(EP, None),
        P(EP, None, TP),
        P(EP, None, TP),
        P(EP, TP, None),
    )
    out_specs = (P(EP, None), P(EP, TP))
    return jax.shard_map(
        on_device, mesh=torus, in_specs=in_specs, out_specs=out_specs, check_vma=False
    )
```

profile of v0, /device:TPU:1, one launch (start us, length us, event | category | flops | bytes accessed | tf_op | source)
XLA Modules:
  0.0 288.2 jit_solution(9969811278149230020)
XLA Ops:
  8.1 1.6 fusion.13
  9.6 0.7 convert_element_type.101
  10.3 1.8 convolution_convert_fusion.3
  12.1 1.8 convolution_convert_fusion.4
  13.9 11.3 %all_gather.12 = bf16[1024,128]{0,1:T(8,128)(2,1)} all-gather(bf16[256,128]{0,1:T(8,128)(2,1)S(1)} %pad_maximum_fusion), channel_id=1, replica_groups=mesh['ep_0'=8,'ep_1'=4,'tp_0'=8,'tp_1'=2] {'ep_1'}, dimensions={0}, use_global_device_ids=true | all-gather | bytes 327680 | tf_op jit(solution)/shard_map/all_gather | solution.py:21
  25.2 0.7 broadcast_multiply_fusion
  25.9 0.8 copy.81
  26.7 0.1 eq.26
  26.8 0.1 reshape.200
  26.9 0.1 copy.86
  27.0 0.1 mul.133
  27.1 0.9 reduce-window.16
  28.0 0.2 slice_reduce_fusion
  28.2 0.1 fusion.49
  28.4 2.9 %scatter_custom_fusion = s32[512]{0:T(512)S(1)} fusion(s32[384]{0:T(512)S(1)} %fusion.55, s32[384]{0:T(512)S(1)} %fusion.51, s32[]{:T(128)} %constant.94.clone.1), kind=kCustom, calls=%fused_computation.97 | custom fusion | bytes 2052 | tf_op jit(solution)/shard_map/scatter | solution.py:164
  31.3 0.8 pad_maximum_fusion.1
  32.1 23.8 %all_gather.15 = bf16[2048,97]{0,1:T(8,128)(2,1)S(1)} all-gather(bf16[128,97]{0,1:T(8,128)(2,1)S(1)} %pad_maximum_fusion.1), channel_id=1, replica_groups=mesh['ep_0'=8,'ep_1'=4,'tp_0'=8,'tp_1'=2] {'tp_0','tp_1'}, dimensions={0}, use_global_device_ids=true | all-gather | bytes 422144 | tf_op jit(solution)/shard_map/all_gather | solution.py:50
  55.8 0.2 fusion.28
  56.0 0.1 broadcast_in_dim.49
  56.1 0.2 fusion.35
  56.3 2.5 gather_fusion
  58.8 1.5 broadcast_select_fusion
  60.3 10.9 %all-to-all-start.2 = ((bf16[32,16,2048]{2,1,0:T(8,128)(2,1)}), bf16[32,16,2048]{2,1,0:T(8,128)(2,1)S(1)}, u32[]{:S(2)}, u32[]{:S(2)}) async-start(bf16[32,16,2048]{2,1,0:T(8,128)(2,1)} %broadcast_select_fusion), calls=%async_computation.2 | async-start | bytes 4194304 | tf_op jit(solution)/shard_map/all_to_all | solution.py:170
  71.2 0.3 reduce-scatter.3.cloned.1.call-start
  71.5 0.8 all-gather.3.cloned.1.call-done
  72.2 7.1 %fusion = f32[256,8192]{1,0:T(8,128)} fusion(f32[8192]{0:T(1024)S(1)} %bitcast.114, bf16[64,2048]{1,0:T(8,128)(2,1)S(1)} %copy-done.5, bf16[8192,128]{0,1:T(8,128)(2,1)} %all-gather.3.cloned.1.call-done, bf16[256,2048]{1,0:T(8,128)(2,1)} %param.15, f32[2048]{0:T(1024)S(1)} %convert_element_type.101, f32[256]{0:T(256)S(1)} %add_rsqrt_fusion.1), kind=kOutput, calls=%fused_computation.6 | convolution fusion | flops 341852160 | bytes 10789888 | tf_op jit(solution)/shard_map/thd,shd->hts/dot_general | solution.py:93
  79.3 7.4 %fusion.9 = f32[32,8,64,128]{3,1,2,0:T(8,128)S(1)} fusion(f32[256,8192]{1,0:T(8,128)} %fusion, s32[256]{0:T(256)S(1)} %iota_add_fusion), kind=kLoop, calls=%fused_computation.17 | loop fusion | flops 18874368 | bytes 16778240
  86.7 4.8 %copy.93 = f32[32,8,64,128]{3,2,1,0:T(8,128)} copy(f32[32,8,64,128]{3,1,2,0:T(8,128)S(1)} %fusion.9) | data formatting | bytes 16777216
  91.6 9.3 %copy.76 = f32[1,256,64,128]{1,2,3,0:T(8,128)} copy(f32[1,256,64,128]{3,2,1,0:T(8,128)} %bitcast.105) | data formatting | bytes 16777216 | tf_op jit(solution)/shard_map/reshape
  100.9 20.8 %all-to-all-done.2 = bf16[32,16,2048]{2,1,0:T(8,128)(2,1)S(1)} async-done(((bf16[32,16,2048]{2,1,0:T(8,128)(2,1)}), bf16[32,16,2048]{2,1,0:T(8,128)(2,1)S(1)}, u32[]{:S(2)}, u32[]{:S(2)}) %all-to-all-start.2) | async-done | bytes 2097184 | tf_op jit(solution)/shard_map/all_to_all | solution.py:170
  121.6 0.7 convolution_minimum_fusion
  122.4 4.7 %fusion.12 = bf16[2048,512]{0,1:T(8,128)(2,1)} fusion(bf16[512,2048]{1,0:T(8,128)(2,1)S(1)} %bitcast.107, bf16[1,128,2048]{2,1,0:T(8,128)(2,1)S(1)} %copy-done, bf16[1,2048,128]{2,1,0:T(8,128)(2,1)} %param.28, f32[512,128]{1,0:T(8,128)S(1)} %convolution_minimum_fusion), kind=kOutput, calls=%fused_computation.20 | convolution fusion | flops 538509312 | bytes 5505024 | tf_op jit(solution)/shard_map/dot_general | solution.py:177
  127.1 3.2 %reshape_reshape.3 = bf16[8,2,128,512]{2,1,0,3:T(2,128)(2,1)S(1)} reshape(bf16[2048,512]{0,1:T(8,128)(2,1)} %fusion.12) | data formatting | bytes 4194304 | tf_op jit(solution)/shard_map/reshape;reshape | solution.py:64
  130.3 4.8 %copy.87 = bf16[8,2,128,512]{3,2,0,1:T(8,128)(2,1)} copy(bf16[8,2,128,512]{2,1,0,3:T(2,128)(2,1)S(1)} %reshape_reshape.3) | data formatting | bytes 4194304 | tf_op jit(solution)/shard_map/reshape;reshape | solution.py:64
  135.2 24.3 %fusion.67 = f32[1,256,64,128]{1,2,3,0:T(8,128)} fusion(f32[1,256,64,128]{1,2,3,0:T(8,128)} %copy.76), kind=kOutput, calls=%fused_computation.110 | output fusion | flops 266338304 | bytes 16777216 | tf_op jit(solution)/shard_map/reduce-window
  159.5 9.0 %copy.77 = f32[1,256,64,128]{3,2,1,0:T(8,128)} copy(f32[1,256,64,128]{1,2,3,0:T(8,128)} %fusion.67) | data formatting | bytes 16777216 | tf_op jit(solution)/shard_map/reduce-window
  168.5 0.8 slice_bitcast_fusion.1
  169.3 0.6 reduce-window.15
  169.9 0.1 copy.78
  170.0 2.3 broadcast.140
  172.3 1.0 copy-done.2
  173.4 18.7 %fusion.23 = bf16[256,64]{0,1:T(8,128)(2,1)S(1)} fusion(f32[32,8,64,128]{3,2,1,0:T(8,128)S(1)} %bitcast.110, f32[32,8,64,128]{3,2,1,0:T(8,128)S(1)} %bitcast.109, f32[256,8192]{1,0:T(8,128)} %fusion, s32[256]{0:T(256)S(1)} %iota_add_fusion, bf16[8192,128]{0,1:T(8,128)(2,1)S(1)} %copy-done.3), kind=kOutput, calls=%fused_computation.39 | convolution fusion | flops 314589184 | bytes 26248192 | tf_op jit(solution)/shard_map/hts,shd->thd/dot_general | solution.py:102
  192.2 0.4 fusion.16
  192.6 1.2 copy.110
  193.9 6.2 %all-to-all-start = ((bf16[16,128,256]{1,2,0:T(8,128)(2,1)}), bf16[16,128,256]{1,2,0:T(8,128)(2,1)S(1)}, u32[]{:S(2)}, u32[]{:S(2)}) async-start(bf16[16,128,256]{1,2,0:T(8,128)(2,1)} %bitcast.102), calls=%async_computation | async-start | bytes 2097152 | tf_op jit(solution)/shard_map/all_to_all | solution.py:33
  200.1 0.5 reduce-scatter.5.cloned.1.call-update
  200.6 29.8 %all-to-all-done = bf16[16,128,256]{1,2,0:T(8,128)(2,1)S(1)} async-done(((bf16[16,128,256]{1,2,0:T(8,128)(2,1)}), bf16[16,128,256]{1,2,0:T(8,128)(2,1)S(1)}, u32[]{:S(2)}, u32[]{:S(2)}) %all-to-all-start) | async-done | bytes 1048608 | tf_op jit(solution)/shard_map/all_to_all | solution.py:33
  230.4 0.1 convert_reduce_fusion
  230.5 0.1 multiply_reduce_fusion.1
  230.7 0.6 broadcast_in_dim.31
  231.3 4.8 %all-to-all-start.1 = ((f32[16,1,256]{2,1,0:T(1,128)}), f32[16,1,256]{2,1,0:T(1,128)S(1)}, u32[]{:S(2)}, u32[]{:S(2)}) async-start(f32[16,1,256]{2,1,0:T(1,128)} %broadcast_in_dim.31), calls=%async_computation.1 | async-start | bytes 32768 | tf_op jit(solution)/shard_map/all_to_all | solution.py:39
  236.1 0.8 dynamic-slice_convert_fusion
  236.9 6.6 %all-to-all-done.1 = f32[16,1,256]{2,1,0:T(1,128)S(1)} async-done(((f32[16,1,256]{2,1,0:T(1,128)}), f32[16,1,256]{2,1,0:T(1,128)S(1)}, u32[]{:S(2)}, u32[]{:S(2)}) %all-to-all-start.1) | async-done | bytes 16416 | tf_op jit(solution)/shard_map/all_to_all | solution.py:39
  243.6 0.7 fusion.46
  244.3 0.1 reduce_sum.72
  244.4 0.1 copy.84
  244.5 1.7 copy.88
  246.2 6.9 %all-to-all-start.3 = ((bf16[128,32,16]{0,2,1:T(8,128)(2,1)}), bf16[128,32,16]{0,2,1:T(8,128)(2,1)S(1)}, u32[]{:S(2)}, u32[]{:S(2)}) async-start(bf16[128,32,16]{0,2,1:T(8,128)(2,1)} %bitcast.21), calls=%async_computation.5 | async-start | bytes 262144 | tf_op jit(solution)/shard_map/all_to_all | solution.py:187
  253.1 0.1 copy.85
  253.3 0.1 copy.89
  253.4 22.5 %all-gather.5.cloned.1.call-done = bf16[256,2048]{1,0:T(8,128)(2,1)} async-done(((bf16[256,128]{1,0:T(8,128)(2,1)}), bf16[256,2048]{1,0:T(8,128)(2,1)}) %all-gather.5.cloned.1.call-update) | async-done | bytes 1048592 | tf_op jit(solution)/shard_map/all_gather | solution.py:152
  275.9 1.4 gather_fusion.1
  277.4 0.9 multiply_reduce_fusion
  278.3 2.3 copy.112
  (45 shorter events, 0.4 us)
Async XLA Ops:
  8.0 114.4 %copy-start = (bf16[1,128,2048]{2,1,0:T(8,128)(2,1)S(1)}, bf16[1,128,2048]{2,1,0:T(8,128)(2,1)}, u32[]{:S(2)}) copy-start(bf16[1,128,2048]{2,1,0:T(8,128)(2,1)} %param.29) | copy-start | bytes 1572868
  8.0 64.2 %all-gather.3.cloned.1.call-start = ((), (), s32[]{:S(2)}) async-start(), calls=%async_computation.6 | async-start | bytes 2359296 | tf_op jit(solution)/shard_map/all_gather | solution.py:21
  58.8 13.5 %copy-start.5 = (bf16[64,2048]{1,0:T(8,128)(2,1)S(1)}, bf16[64,2048]{1,0:T(8,128)(2,1)}, u32[]{:S(2)}) copy-start(bf16[64,2048]{1,0:T(8,128)(2,1)} %param.17) | copy-start | bytes 786436
  58.8 13.5 %copy-start.7 = (f32[1,8192]{1,0:T(1,128)S(1)}, f32[1,8192]{1,0:T(1,128)}, u32[]{:S(2)}) copy-start(f32[1,8192]{1,0:T(1,128)} %param.20) | copy-start | bytes 98308
  60.3 61.3 %all-to-all-start.2 = ((bf16[32,16,2048]{2,1,0:T(8,128)(2,1)}), bf16[32,16,2048]{2,1,0:T(8,128)(2,1)S(1)}, u32[]{:S(2)}, u32[]{:S(2)}) async-start(bf16[32,16,2048]{2,1,0:T(8,128)(2,1)} %broadcast_select_fusion), calls=%async_computation.2 | async-start | bytes 4194304 | tf_op jit(solution)/shard_map/all_to_all | solution.py:170
  71.2 128.9 %reduce-scatter.3.cloned.1.call-start = ((), (), s32[]{:S(2)}) async-start(), calls=%async_computation.8 | async-start | bytes 3145728 | tf_op jit(solution)/shard_map/reduce_scatter | solution.py:65
  91.6 30.0 %copy-start.4 = (bf16[1,2048,128]{2,1,0:T(8,128)(2,1)S(1)}, bf16[1,2048,128]{2,1,0:T(8,128)(2,1)}, u32[]{:S(2)}) copy-start(bf16[1,2048,128]{2,1,0:T(8,128)(2,1)} %param.27) | copy-start | bytes 1572868
  159.5 12.9 %copy-start.3 = (bf16[8192,128]{0,1:T(8,128)(2,1)S(1)}, bf16[8192,128]{0,1:T(8,128)(2,1)}, u32[]{:S(2)}) copy-start(bf16[8192,128]{0,1:T(8,128)(2,1)} %all-gather.3.cloned.1.call-done) | copy-start | bytes 6291460
  170.0 3.4 %copy-start.2 = (f32[1,256,64,128]{3,2,1,0:T(8,128)S(1)}, f32[1,256,64,128]{3,2,1,0:T(8,128)}, u32[]{:S(2)}) copy-start(f32[1,256,64,128]{3,2,1,0:T(8,128)} %copy.77) | copy-start | bytes 25165828
  173.4 18.7 %copy-start.6 = (bf16[64,2048]{1,0:T(8,128)(2,1)S(1)}, bf16[64,2048]{1,0:T(8,128)(2,1)}, u32[]{:S(2)}) copy-start(bf16[64,2048]{1,0:T(8,128)(2,1)} %param.21) | copy-start | bytes 786436
  173.4 107.2 %copy-start.1 = (bf16[1,128,2048]{2,1,0:T(8,128)(2,1)S(1)}, bf16[1,128,2048]{2,1,0:T(8,128)(2,1)}, u32[]{:S(2)}) copy-start(bf16[1,128,2048]{2,1,0:T(8,128)(2,1)} %param.29) | copy-start | bytes 1572868
  192.1 61.0 %copy-start.8 = (s32[96,4]{0,1:T(4,128)S(1)}, s32[96,4]{0,1:T(4,128)}, u32[]{:S(2)}) copy-start(s32[96,4]{0,1:T(4,128)} %param.25) | copy-start | bytes 4612
  192.1 61.1 %copy-start.9 = (f32[96,4]{0,1:T(4,128)S(1)}, f32[96,4]{0,1:T(4,128)}, u32[]{:S(2)}) copy-start(f32[96,4]{0,1:T(4,128)} %param.26) | copy-start | bytes 4612
  193.9 36.5 %all-to-all-start = ((bf16[16,128,256]{1,2,0:T(8,128)(2,1)}), bf16[16,128,256]{1,2,0:T(8,128)(2,1)S(1)}, u32[]{:S(2)}, u32[]{:S(2)}) async-start(bf16[16,128,256]{1,2,0:T(8,128)(2,1)} %bitcast.102), calls=%async_computation | async-start | bytes 2097152 | tf_op jit(solution)/shard_map/all_to_all | solution.py:33
  200.0 44.5 %reduce-scatter.5.cloned.1.call-start = ((), (), s32[]{:S(2)}) async-start(), calls=%async_computation.9 | async-start | bytes 1179648 | tf_op jit(solution)/shard_map/reduce_scatter | solution.py:66
  231.3 12.2 %all-to-all-start.1 = ((f32[16,1,256]{2,1,0:T(1,128)}), f32[16,1,256]{2,1,0:T(1,128)S(1)}, u32[]{:S(2)}, u32[]{:S(2)}) async-start(f32[16,1,256]{2,1,0:T(1,128)} %broadcast_in_dim.31), calls=%async_computation.1 | async-start | bytes 32768 | tf_op jit(solution)/shard_map/all_to_all | solution.py:39
  236.1 39.8 %all-gather.5.cloned.1.call-start = ((), (), s32[]{:S(2)}) async-start(), calls=%async_computation.7 | async-start | bytes 1114112 | tf_op jit(solution)/shard_map/all_gather | solution.py:152
  246.2 29.8 %all-to-all-start.3 = ((bf16[128,32,16]{0,2,1:T(8,128)(2,1)}), bf16[128,32,16]{0,2,1:T(8,128)(2,1)S(1)}, u32[]{:S(2)}, u32[]{:S(2)}) async-start(bf16[128,32,16]{0,2,1:T(8,128)(2,1)} %bitcast.21), calls=%async_computation.5 | async-start | bytes 262144 | tf_op jit(solution)/shard_map/all_to_all | solution.py:187
Sparse Core Ops, SparseCore 0:
  25.3 46.8 all-gather.2
  244.4 31.4 all-gather.4
Sparse Core Ops, SparseCore 1:
  135.2 15.2 reduce-scatter.2
  203.3 40.2 reduce-scatter.4
where the time goes:
time: 294 us; the launch traced here: 288 us
  waiting for transfers between devices  81 us (28%)
  local copies, waits for them, and re-layouts  50.1 us (17%)
  other arithmetic  41.7 us (14%)
  matrix products  35.2 us (12%)
  blocking collectives  35 us (12%)
  starting transfers between devices  29.2 us (10%)
  between operations  16 us (5%)
    all_to_all x1, waiting for transfers between devices, sent_and_summed(): lax.all_to_all(split_up(value, dim, devices), axis, 0, 0, tiled=True)  29.8 us
    another operation x4, other arithmetic  25.8 us
    all_gather x1, blocking collectives, gather_turned(): out = lax.all_gather(both, axis, axis=0, tiled=True)  23.8 us
    all_gather x1, waiting for transfers between devices, on_device(): mix_out = lax.all_gather(own_columns, TP, axis=1, tiled=True)  22.5 us
    all_to_all x1, waiting for transfers between devices, on_device(): lax.all_to_all(outgoing, EP, split_axis=0, concat_axis=0, tiled=True)  20.8 us
    dot_general x1, matrix products, stick_terms(): jnp.einsum('hts,shd->thd', weights, value_rows, preferred_element_type=jn...  18.7 us
    another operation x6, local copies, waits for them, and re-layouts  12.5 us
    all_gather x1, blocking collectives, gathered_by_axis(): out = lax.all_gather(out, axes[number], axis=dim, tiled=True)  11.3 us
  transfers between devices with their start and end apart: 8, of which 5 were waited for; matrix products, arithmetic and copies ran while one was open for 35% of the time, Pallas kernels for 0%

commit v1 on v0

v1 whole, which is shorter than its diff:
```python
import math

import jax
import jax.numpy as jnp
from jax import lax
from jax.experimental import pallas as pl
from jax.experimental.pallas import tpu as pltpu
from jax.sharding import Mesh
from jax.sharding import PartitionSpec as P

EP = ("ep_0", "ep_1")
TP = ("tp_0", "tp_1")
Z, X, Y, C = 8, 4, 8, 2
N_EP, N_TP = Z * X, Y * C

EPSILON = 1e-06
CLAMP_LIMIT = 7.0
SILU_SHARPNESS = 1.702
LOG2E = math.log2(math.e)

D = 2048
HEAD = 64
ROWS = 256
HALF = ROWS // 2
TOK = 96
CAP = 16
SLOTS = N_EP * CAP
COLS = D // N_TP
GAIN_ROWS = 16

F32 = jnp.float32
BF16 = jnp.bfloat16
MESH = pl.DeviceIdType.MESH
NT = (((1,), (1,)), ((), ()))
TN = (((0,), (0,)), ((), ()))


def dot(a, b):
    return jnp.dot(a, b, preferred_element_type=F32)


def iota(shape, dim):
    return lax.broadcasted_iota(jnp.int32, shape, dim)


def split_two(value):
    high = value.astype(BF16)
    return high, (value - high.astype(F32)).astype(BF16)


def body(
    mix_rows, mix_gain, w_query, w_key, w_value, key_offset, w_out, out_gain, exp_rows, exp_gain,
    routes, route_weight, w_gate, w_up, w_down,
    mix_out, exp_out,
    rows, wqkv, q_pad, kvg, acc, carry, tri,
    picks, weight_hi, weight_lo, sent, grid, wgu, gu, ssq, hid, wd_own, wd, wo_own, wo,
    att, out_acc, cols, result, returned,
    load_sem, disp_send, disp_recv, kva_send, kva_recv, kvb_send, kvb_recv,
    grid_send, grid_recv, hid_send, hid_recv, wd_send, wd_recv, wo_send, wo_recv,
    att_send, att_recv, cols_send, cols_recv, ret_send, ret_recv,
):
    z, x = lax.axis_index("ep_0"), lax.axis_index("ep_1")
    y, c = lax.axis_index("tp_0"), lax.axis_index("tp_1")
    ep, tp = z * X + x, y * C + c
    partner = {"tp_1": 1 - c}
    y_up, y_down = {"tp_0": lax.rem(y + 1, Y)}, {"tp_0": lax.rem(y + Y - 1, Y)}
    z_up, z_down = {"ep_0": lax.rem(z + 1, Z)}, {"ep_0": lax.rem(z + Z - 1, Z)}

    def ep_peer(distance):
        other = lax.rem(ep + distance, N_EP)
        return other, {"ep_0": other // X, "ep_1": lax.rem(other, X)}

    def tp_peer(distance):
        other = lax.rem(tp + distance, N_TP)
        return other, {"tp_0": other // C, "tp_1": lax.rem(other, C)}

    def remote(src, dst, send_sem, recv_sem, device):
        return pltpu.make_async_remote_copy(
            src_ref=src, dst_ref=dst, send_sem=send_sem, recv_sem=recv_sem,
            device_id=device, device_id_type=MESH,
        )

    loads = [
        (mix_rows, rows),
        (w_query, wqkv.at[pl.ds(0, HEAD)]),
        (w_key, wqkv.at[pl.ds(2 * HEAD, HEAD)]),
        (w_value, wqkv.at[pl.ds(3 * HEAD, HEAD)]),
        (w_out, wo_own),
        (w_down.at[0], wd_own),
        (w_gate.at[0], wgu.at[:, pl.ds(0, COLS)]),
        (w_up.at[0], wgu.at[:, pl.ds(COLS, COLS)]),
    ]
    loads = [pltpu.make_async_copy(a, b, load_sem.at[n]) for n, (a, b) in enumerate(loads)]
    for load in loads:
        load.start()

    barrier = pltpu.get_barrier_semaphore()

    @pl.loop(1, N_EP)
    def _(distance):
        pl.semaphore_signal(barrier, 1, device_id=ep_peer(distance)[1], device_id_type=MESH)

    @pl.loop(1, N_TP)
    def _(distance):
        pl.semaphore_signal(barrier, 1, device_id=tp_peer(distance)[1], device_id_type=MESH)

    lane = iota((TOK, 128), 1)
    member = jnp.zeros((TOK, 128), F32)
    weight = jnp.zeros((TOK, 128), F32)
    for k in range(routes.shape[1]):
        hit = routes[:, k : k + 1] == lane
        member = member + jnp.where(hit, 1.0, 0.0)
        weight = weight + jnp.where(hit, route_weight[:, k : k + 1], 0.0)
    member = member.astype(BF16)
    earlier = jnp.where(iota((TOK, TOK), 1) < iota((TOK, TOK), 0), 1.0, 0.0).astype(BF16)
    before = dot(earlier, member).astype(BF16)
    spread = jnp.where(iota((128, SLOTS), 1) // CAP == iota((128, SLOTS), 0), 1.0, 0.0).astype(BF16)
    place = lax.rem(iota((TOK, SLOTS), 1), CAP).astype(F32)
    chosen = (dot(member, spread) > 0.5) & (dot(before, spread) == place)
    picks[...] = jnp.where(chosen, 1.0, 0.0).astype(BF16)
    high, low = split_two(weight)
    weight_hi[...] = jnp.where(chosen, dot(high, spread), 0.0).astype(BF16)
    weight_lo[...] = jnp.where(chosen, dot(low, spread), 0.0).astype(BF16)
    sent[...] = lax.dot_general(picks[...], exp_rows[...], TN, preferred_element_type=F32).astype(BF16)
    own_slots = pl.ds(pl.multiple_of(ep * CAP, CAP), CAP)
    grid[tp, own_slots, :] = sent[own_slots, :]
    grid[tp, pl.ds(SLOTS, GAIN_ROWS), :] = jnp.broadcast_to(exp_gain[...], (GAIN_ROWS, COLS))

    wqkv[pl.ds(HEAD, HEAD), :] = jnp.zeros((HEAD, D), BF16)
    tri[...] = jnp.where(
        (iota((256, 256), 1) >= HALF)
        | (lax.rem(iota((256, 256), 0), HALF) >= iota((256, 256), 1)), 1.0, 0.0,
    ).astype(BF16)
    loads[0].wait()
    gain = mix_gain[...].astype(F32)

    @pl.loop(0, ROWS // 32)
    def _(n):
        at = pl.ds(pl.multiple_of(n * 32, 32), 32)
        numbers = rows[at, :].astype(F32)
        factor = lax.rsqrt(jnp.mean(numbers * numbers, axis=-1, keepdims=True) + EPSILON)
        rows[at, :] = (numbers * factor * gain).astype(BF16)

    for load in loads[1:4]:
        load.wait()
    projected = lax.dot_general(rows[...], wqkv[...], NT, preferred_element_type=F32).astype(BF16)
    q_pad[...] = projected[:, : 2 * HEAD]
    kvg[ep] = projected[:, 2 * HEAD :]
    loads[4].wait()
    loads[5].wait()

    pl.semaphore_wait(barrier, N_EP - 1 + N_TP - 1)

    part_a, part_b = pl.ds(0, HALF), pl.ds(HALF, HALF)

    def send_a(slot, device):
        part = kvg.at[slot, part_a]
        remote(part, part, kva_send, kva_recv.at[slot], device).start()

    def send_b(slot, device):
        part = kvg.at[slot, part_b]
        remote(part, part, kvb_send, kvb_recv.at[slot], device).start()

    def wait_a(slot):
        part = kvg.at[slot, part_a]
        remote(part, part, kva_send, kva_recv.at[slot], partner).wait_recv()

    def wait_b(slot):
        part = kvg.at[slot, part_b]
        remote(part, part, kvb_send, kvb_recv.at[slot], partner).wait_recv()

    def x_peer(distance):
        return lax.rem(x + distance, X)

    def send_b_across(slot):
        for distance in range(1, X):
            send_b(slot, {"ep_1": x_peer(distance)})

    def disp_copy(distance):
        other, device = ep_peer(distance)
        return remote(
            sent.at[pl.ds(pl.multiple_of(other * CAP, CAP), CAP)],
            grid.at[tp, own_slots],
            disp_send, disp_recv, device,
        )

    @pl.loop(1, N_EP)
    def _(distance):
        disp_copy(distance).start()

    for distance in range(1, X):
        send_a(ep, {"ep_1": x_peer(distance)})
    send_b(ep, z_up)
    send_b(ep, z_down)
    send_a(ep, z_up)
    send_a(ep, z_down)
    send_b_across(ep)

    def columns_of(other):
        return pl.ds(pl.multiple_of(other * COLS, COLS), COLS)

    own_columns = columns_of(tp)

    @pl.loop(1, N_TP)
    def _(distance):
        other, device = tp_peer(distance)
        remote(wd_own.at[:, columns_of(other)], wd.at[tp], wd_send, wd_recv, device).start()

    @pl.loop(1, N_TP)
    def _(distance):
        other, device = tp_peer(distance)
        remote(wo_own.at[:, columns_of(other)], wo.at[tp], wo_send, wo_recv, device).start()

    wd[tp] = wd_own[:, own_columns]
    wo[tp] = wo_own[:, own_columns]

    for distance in range(1, X):
        slot = z * X + x_peer(distance)
        wait_a(slot)
        send_a(slot, z_up)
        send_a(slot, z_down)

    def attend(block, diagonal):
        kv = kvg[block]
        offsets = key_offset[:, pl.ds(pl.multiple_of(block * ROWS, ROWS), ROWS)] * LOG2E
        scores = lax.dot_general(q_pad[...], kv, NT, preferred_element_type=F32)
        scores = scores * (LOG2E / math.sqrt(HEAD)) + offsets
        drop = jnp.maximum(jnp.log2(1.0 + jnp.exp2(jnp.minimum(scores, 100.0))), scores)
        if diagonal:
            visible = iota((ROWS, ROWS), 1) < iota((ROWS, ROWS), 0)
            drop = jnp.where(visible, drop, 0.0)
        for half in (1, 0):
            at = slice(half * HALF, (half + 1) * HALF)
            totals = dot(jnp.concatenate(split_two(drop[:, at]), axis=1), tri[...])
            weights = jnp.exp2(scores[:, at] - totals[:, :HALF] - carry[...])
            if diagonal:
                weights = jnp.where(visible[:, at], weights, 0.0)
            acc[...] += dot(weights.astype(BF16), kv[at, :])
            carry[...] += totals[:, HALF:]

    def attend_row(back):
        row = z - back

        @pl.when(row >= 0)
        def _():
            @pl.loop(0, X)
            def _(n):
                attend(row * X + X - 1 - n, False)

    acc[...] = jnp.zeros(acc.shape, F32)
    carry[...] = jnp.zeros(carry.shape, F32)
    attend(ep, True)
    for distance in range(1, X):
        wait_b(z * X + x_peer(distance))

    @pl.loop(0, x)
    def _(n):
        attend(ep - 1 - n, False)

    def ring(buffer, send_sem, recv_sem):
        def send(slot, device):
            block = buffer.at[slot]
            remote(block, block, send_sem, recv_sem.at[slot], device).start()

        def wait(slot):
            block = buffer.at[slot]
            remote(block, block, send_sem, recv_sem.at[slot], partner).wait_recv()

        def start():
            for device in (y_up, y_down, partner):
                send(tp, device)

        def step(k):
            slot = lax.rem(y + Y - k, Y) * C + c
            wait(slot)
            if k < Y // 2:
                send(slot, y_up)
            send(slot, partner)
            if k < Y // 2:
                slot = lax.rem(y + k, Y) * C + c
                wait(slot)
                if k < Y // 2 - 1:
                    send(slot, y_down)
                send(slot, partner)

        def finish():
            @pl.loop(0, Y)
            def _(n):
                wait(n * C + 1 - c)

        def drain():
            blocks = buffer.at[pl.ds(0, N_TP - 1)]
            remote(blocks, blocks, send_sem, recv_sem.at[0], partner).wait_send()

        return start, step, finish, drain

    grid_ring = ring(grid, grid_send, grid_recv)
    hid_ring = ring(hid, hid_send, hid_recv)
    att_ring = ring(att, att_send, att_recv)
    cols_ring = ring(cols, cols_send, cols_recv)

    arrived = grid.at[tp, pl.ds(0, SLOTS - CAP)]
    remote(arrived, arrived, disp_send, disp_recv, partner).wait_recv()
    grid_ring[0]()

    def kv_step(k):
        row = lax.rem(z + Z - k, Z) * X
        for distance in range(X):
            slot = row + x_peer(distance)
            wait_a(slot)
            if k < Z // 2:
                send_a(slot, z_up)
        slot = row + x
        wait_b(slot)
        if k < Z // 2:
            send_b(slot, z_up)
        send_b_across(slot)
        if k < Z // 2:
            row = lax.rem(z + k, Z) * X
            for distance in range(X):
                slot = row + x_peer(distance)
                wait_a(slot)
                if k < Z // 2 - 1:
                    send_a(slot, z_down)
            slot = row + x
            wait_b(slot)
            if k < Z // 2 - 1:
                send_b(slot, z_down)
            send_b_across(slot)

    def kv_finish(k):
        row = lax.rem(z + Z - k, Z) * X
        for distance in range(1, X):
            wait_b(row + x_peer(distance))

    for k in range(1, 5):
        kv_step(k)
        grid_ring[1](k)
        if k > 1:
            kv_finish(k - 1)
            attend_row(k - 1)

    grid_ring[2]()
    loads[6].wait()
    loads[7].wait()
    gu[...] = jnp.zeros(gu.shape, F32)
    ssq[...] = jnp.zeros(ssq.shape, F32)

    @pl.loop(0, N_TP // 2)
    def _(n):
        scaled = []
        for m in range(2):
            numbers = grid[2 * n + m, pl.ds(0, SLOTS), :].astype(F32)
            gains = grid[2 * n + m, pl.ds(SLOTS, GAIN_ROWS), :][:1].astype(F32)
            ssq[...] += numbers * numbers
            scaled.append((numbers * gains).astype(BF16))
        part = wgu[pl.ds(pl.multiple_of(n * 2 * COLS, 2 * COLS), 2 * COLS), :]
        gu[...] += dot(jnp.concatenate(scaled, axis=1), part)

    factor = lax.rsqrt(jnp.sum(ssq[...], axis=1, keepdims=True) / D + EPSILON)
    gate_part = jnp.minimum(gu[:, :COLS] * factor, CLAMP_LIMIT)
    up_part = jnp.clip(gu[:, COLS:] * factor, -CLAMP_LIMIT, CLAMP_LIMIT)
    hid[tp] = (
        (up_part + 1.0) * (gate_part * jax.nn.sigmoid(SILU_SHARPNESS * gate_part))
    ).astype(BF16)
    hid_ring[0]()

    for k in range(4, 8):
        kv_finish(k)
        attend_row(k)
    first = pltpu.roll(acc[pl.ds(0, HALF), :], HEAD, 1)
    att[tp] = jnp.where(iota((HALF, 128), 1) < HEAD, first, acc[pl.ds(HALF, HALF), :]).astype(BF16)
    att_ring[0]()
    for k in range(1, 5):
        att_ring[1](k)
        hid_ring[1](k)
    att_ring[2]()

    pieces = wo.at[pl.ds(0, N_TP - 1)]
    remote(pieces, pieces, wo_send, wo_recv, partner).wait_recv()
    out_acc[...] = jnp.zeros(out_acc.shape, F32)

    @pl.loop(0, N_TP)
    def _(n):
        piece = wo[n]
        zeros = jnp.zeros_like(piece)
        twice = jnp.concatenate(
            [jnp.concatenate([piece, zeros], axis=1), jnp.concatenate([zeros, piece], axis=1)], axis=0
        )
        out_acc[...] += dot(att[n], twice)

    cols[tp, pl.ds(0, HALF), :] = out_acc[:, :COLS].astype(BF16)
    cols[tp, pl.ds(HALF, HALF), :] = out_acc[:, COLS:].astype(BF16)
    cols_ring[0]()

    hid_ring[2]()
    pieces = wd.at[pl.ds(0, N_TP - 1)]
    remote(pieces, pieces, wd_send, wd_recv, partner).wait_recv()
    gu[:, :COLS] = jnp.zeros((SLOTS, COLS), F32)

    @pl.loop(0, N_TP // 2)
    def _(n):
        left = jnp.concatenate([hid[2 * n], hid[2 * n + 1]], axis=1)
        right = jnp.concatenate([wd[2 * n], wd[2 * n + 1]], axis=0)
        gu[:, :COLS] += dot(left, right)

    result[...] = gu[:, :COLS].astype(BF16)
    returned[own_slots, :] = result[own_slots, :]

    @pl.loop(1, N_EP)
    def _(distance):
        other, device = ep_peer(distance)
        remote(
            result.at[pl.ds(pl.multiple_of(other * CAP, CAP), CAP)],
            returned.at[own_slots],
            ret_send, ret_recv, device,
        ).start()

    for k in range(1, 5):
        cols_ring[1](k)
    cols_ring[2]()

    squares = jnp.zeros((ROWS, COLS), F32)
    for n in range(N_TP):
        numbers = cols[n].astype(F32)
        squares = squares + numbers * numbers
    factor = lax.rsqrt(jnp.sum(squares, axis=1, keepdims=True) / D + EPSILON)
    for n in range(N_TP):
        at = slice(n * COLS, (n + 1) * COLS)
        mix_out[:, at] = (cols[n].astype(F32) * factor * out_gain[:, at].astype(F32)).astype(BF16)

    arrived = returned.at[pl.ds(0, SLOTS - CAP)]
    remote(arrived, arrived, ret_send, ret_recv, partner).wait_recv()
    exp_out[...] = (dot(weight_hi[...], returned[...]) + dot(weight_lo[...], returned[...])).astype(BF16)

    part = kvg.at[pl.ds(0, N_EP - 1), part_a]
    remote(part, part, kva_send, kva_recv.at[0], partner).wait_send()
    remote(part, part, kvb_send, kvb_recv.at[0], partner).wait_send()
    part = sent.at[pl.ds(0, SLOTS - CAP)]
    remote(part, part, disp_send, disp_recv, partner).wait_send()
    remote(part, part, ret_send, ret_recv, partner).wait_send()
    part = wd.at[pl.ds(0, N_TP - 1)]
    remote(part, part, wd_send, wd_recv, partner).wait_send()
    part = wo.at[pl.ds(0, N_TP - 1)]
    remote(part, part, wo_send, wo_recv, partner).wait_send()
    for one in (grid_ring, hid_ring, att_ring, cols_ring):
        one[3]()


def on_device(*args):
    (mix_rows, mix_gain, w_query, w_key, w_value, key_offset, w_out, out_gain, exp_rows, exp_gain,
     routes, route_weight, w_gate, w_up, w_down) = args
    vmem, hbm = pl.BlockSpec(memory_space=pltpu.VMEM), pl.BlockSpec(memory_space=pl.ANY)
    dma = pltpu.SemaphoreType.DMA
    return pl.pallas_call(
        body,
        out_shape=(
            jax.ShapeDtypeStruct((ROWS, D), BF16),
            jax.ShapeDtypeStruct((TOK, COLS), BF16),
        ),
        in_specs=[
            hbm, vmem, hbm, hbm, hbm, vmem, hbm, vmem, vmem, vmem, vmem, vmem, hbm, hbm, hbm,
        ],
        out_specs=(vmem, vmem),
        scratch_shapes=[
            pltpu.VMEM((ROWS, D), BF16),
            pltpu.VMEM((4 * HEAD, D), BF16),
            pltpu.VMEM((ROWS, 128), BF16),
            pltpu.VMEM((N_EP, ROWS, 128), BF16),
            pltpu.VMEM((ROWS, 128), F32),
            pltpu.VMEM((ROWS, 128), F32),
            pltpu.VMEM((256, 256), BF16),
            pltpu.VMEM((TOK, SLOTS), BF16),
            pltpu.VMEM((TOK, SLOTS), BF16),
            pltpu.VMEM((TOK, SLOTS), BF16),
            pltpu.VMEM((SLOTS, COLS), BF16),
            pltpu.VMEM((N_TP, SLOTS + GAIN_ROWS, COLS), BF16),
            pltpu.VMEM((D, 2 * COLS), BF16),
            pltpu.VMEM((SLOTS, 2 * COLS), F32),
            pltpu.VMEM((SLOTS, COLS), F32),
            pltpu.VMEM((N_TP, SLOTS, COLS), BF16),
            pltpu.VMEM((COLS, D), BF16),
            pltpu.VMEM((N_TP, COLS, COLS), BF16),
            pltpu.VMEM((HEAD, D), BF16),
            pltpu.VMEM((N_TP, HEAD, COLS), BF16),
            pltpu.VMEM((N_TP, HALF, 128), BF16),
            pltpu.VMEM((HALF, 2 * COLS), F32),
            pltpu.VMEM((N_TP, ROWS, COLS), BF16),
            pltpu.VMEM((SLOTS, COLS), BF16),
            pltpu.VMEM((SLOTS, COLS), BF16),
            dma((8,)),
            dma(()), dma(()),
            dma(()), dma((N_EP,)), dma(()), dma((N_EP,)),
            dma(()), dma((N_TP,)), dma(()), dma((N_TP,)),
            dma(()), dma(()), dma(()), dma(()),
            dma(()), dma((N_TP,)), dma(()), dma((N_TP,)),
            dma(()), dma(()),
        ],
        compiler_params=pltpu.CompilerParams(
            collective_id=0, has_side_effects=True, vmem_limit_bytes=60 * 1024 * 1024
        ),
    )(
        mix_rows, mix_gain.reshape(1, D), w_query, w_key, w_value, key_offset, w_out,
        out_gain.reshape(1, D), exp_rows, exp_gain.reshape(1, COLS), routes, route_weight,
        w_gate, w_up, w_down,
    )


def solution(mesh):
    torus = Mesh(mesh.devices.reshape(Z, X, Y, C), EP + TP)
    in_specs = (
        P(EP, None),
        P(),
        P(TP, None),
        P(TP, None),
        P(TP, None),
        P(TP, None),
        P(TP, None),
        P(),
        P(EP, TP),
        P(TP),
        P(EP, None),
        P(EP, None),
        P(EP, None, TP),
        P(EP, None, TP),
        P(EP, TP, None),
    )
    out_specs = (P(EP, None), P(EP, TP))
    return jax.shard_map(
        on_device, mesh=torus, in_specs=in_specs, out_specs=out_specs, check_vma=False
    )
```

time: 294 us -> 103 us (0.35); the launches traced: 288 us -> 103 us
  Pallas kernels: 0 us -> 95.8 us
  waiting for transfers between devices: 81 us -> 0 us
  local copies, waits for them, and re-layouts: 50.1 us -> 6.34 us
  other arithmetic: 41.7 us -> 0 us
  matrix products: 35.2 us -> 0 us
  blocking collectives: 35 us -> 0 us
  starting transfers between devices: 29.2 us -> 0 us
  between operations: 16 us -> 0.66 us
    pallas_call x0 -> x1, Pallas kernels: none -> 95.8 us  [on_device(): pl.pallas_call(body, out_shape=(jax.ShapeDtypeStruct((ROWS, D), BF16), ja...]
    all_to_all x4 -> x0, waiting for transfers between devices: 57.2 us -> none  [the longest x1 29.8 us: sent_and_summed(): lax.all_to_all(split_up(value, dim, devices), axis, 0, 0, tiled=True)]
    dot_general x7 -> x0, matrix products: 35.2 us -> none  [the longest x1 18.7 us: stick_terms(): jnp.einsum('hts,shd->thd', weights, value_rows, preferred_element_type=jn...]
    all_gather x2 -> x0, blocking collectives: 35 us -> none  [the longest x1 23.8 us: gather_turned(): out = lax.all_gather(both, axis, axis=0, tiled=True)]
    all_to_all x4 -> x0, starting transfers between devices: 28.8 us -> none  [the longest x1 10.9 us: on_device(): lax.all_to_all(outgoing, EP, split_axis=0, concat_axis=0, tiled=True)]
    another operation x4 -> x0, other arithmetic: 25.8 us -> none
    all_gather x2 -> x0, waiting for transfers between devices: 23.3 us -> none  [the longest x1 22.5 us: on_device(): mix_out = lax.all_gather(own_columns, TP, axis=1, tiled=True)]
    another operation x8 -> x0, local copies, waits for them, and re-layouts: 20.5 us -> none
  transfers between devices with their start and end apart: 8 -> 0, of which waited for: 5 -> 0; matrix products, arithmetic and copies ran while one was open for 35% -> 0% of each run, Pallas kernels for 0% -> 0%
where the time goes in v1:
time: 103 us
  Pallas kernels  95.8 us (93%)
  local copies, waits for them, and re-layouts  6.34 us (6%)
    pallas_call x1, Pallas kernels, on_device(): pl.pallas_call(body, out_shape=(jax.ShapeDtypeStruct((ROWS, D), BF16), ja...  95.8 us
    unnamed x12, local copies, waits for them, and re-layouts  4.45 us

profile of v1, /device:TPU:1, one launch (start us, length us, event | category | flops | bytes accessed | tf_op | source)
XLA Modules:
  0.0 102.8 jit_solution(9213566817186311176)
XLA Ops:
  0.6 0.0 copy-start.1
  0.6 1.3 %reshape.13.mix_gain = bf16[1,2048]{1,0:T(2,128)(2,1)} reshape(bf16[2048]{0:T(1024)(128)(2,1)} %param.16) | data formatting | bytes 8192 | tf_op jit(solution)/shard_map/reshape | solution.py:503
  1.9 0.0 copy-done.1
  1.9 0.0 copy-start.2
  1.9 0.6 reshape.14.out_gain
  2.5 0.1 copy-done.2
  2.6 0.0 copy-start.3
  2.6 0.7 copy.17.routes
  3.4 0.0 copy-done.3
  3.4 0.7 copy.18.route_weight
  4.1 95.8 %shard_map.158 = (bf16[256,2048]{1,0:T(8,128)(2,1)}, bf16[96,128]{1,0:T(8,128)(2,1)}) custom-call(bf16[256,2048]{1,0:T(8,128)(2,1)} %mix_rows.1, bf16[1,2048]{1,0:T(2,128)(2,1)} %reshape.13.mix_gain, bf16[64,2048]{1,0:T(8,128)(2,1)} %w_query.1, bf16[64,2048]{1,0:T(8,128)(2,1)} %w_key.1, bf16[64,2048]{1,0:T(8,128)(2,1)} %w_value.1, f32[1,8192]{1,0:T(1,128)} %key_offset.1, ...), custom_call_target="tpu_custom_call" | custom-call | tf_op jit(solution)/shard_map/pallas_call | solution.py:455
  99.9 0.0 copy-start
  99.9 2.3 %copy.21 = bf16[256,2048]{1,0:T(8,128)(2,1)} copy(bf16[256,2048]{1,0:T(8,128)(2,1)} %get-tuple-element.4) | data formatting | bytes 2097152
  102.2 0.0 copy-done
  102.2 0.6 copy.22
Async XLA Ops:
  0.6 1.3 %copy-start.1 = (bf16[2048]{0:T(1024)(128)(2,1)S(1)}, bf16[2048]{0:T(1024)(128)(2,1)}, u32[]{:S(2)}) copy-start(bf16[2048]{0:T(1024)(128)(2,1)} %param.22) | copy-start | bytes 12292
  1.9 0.7 copy-start.2
  2.6 0.7 copy-start.3
  99.9 2.3 %copy-start = (bf16[96,128]{1,0:T(8,128)(2,1)S(1)}, bf16[96,128]{1,0:T(8,128)(2,1)}, u32[]{:S(2)}) copy-start(bf16[96,128]{1,0:T(8,128)(2,1)} %get-tuple-element.5) | copy-start | bytes 73732

commit v2 on v1

v2 whole, which is shorter than its diff:
```python
import math

import jax
import jax.numpy as jnp
from jax import lax
from jax.experimental import pallas as pl
from jax.experimental.pallas import tpu as pltpu
from jax.sharding import Mesh
from jax.sharding import PartitionSpec as P

EP = ("ep_0", "ep_1")
TP = ("tp_0", "tp_1")
Z, X, Y, C = 8, 4, 8, 2
N_EP, N_TP = Z * X, Y * C

EPSILON = 1e-06
CLAMP_LIMIT = 7.0
SILU_SHARPNESS = 1.702
LOG2E = math.log2(math.e)

D = 2048
HEAD = 64
ROWS = 256
HALF = ROWS // 2
TOK = 96
CAP = 16
SLOTS = N_EP * CAP
COLS = D // N_TP
GAIN_ROWS = 16
GRID_PIECES, ATT_PIECES, COLS_PIECES, SUM_PIECES = 4, 2, 2, 2
SUM_ROWS = SLOTS // SUM_PIECES

F32 = jnp.float32
BF16 = jnp.bfloat16
MESH = pl.DeviceIdType.MESH
NT = (((1,), (1,)), ((), ()))
TN = (((0,), (0,)), ((), ()))


def dot(a, b):
    return jnp.dot(a, b, preferred_element_type=F32)


def iota(shape, dim):
    return lax.broadcasted_iota(jnp.int32, shape, dim)


def split_two(value):
    high = value.astype(BF16)
    return high, (value - high.astype(F32)).astype(BF16)


def body(
    mix_rows, mix_gain, w_query, w_key, w_value, key_offset, w_out, out_gain, exp_rows, exp_gain,
    routes, route_weight, w_gate, w_up, w_down,
    mix_out, exp_out,
    gain_in, gain_out, offset, tokens, token_gain, route, route_scale,
    rows, wqkv, q_pad, kvg, acc, carry, far, drops, tri,
    picks, weight_hi, weight_lo, sent, grid, gains, wgu, gu, ssq, wd_own, wo_own, wo, wo_wide,
    part, pin, up_out, up_in, down_out, down_in,
    att, cols, result, returned,
    load_sem, disp_send, disp_recv, kva_send, kva_recv, kvb_send, kvb_recv,
    grid_send, grid_recv, gain_send, gain_recv, wo_send, wo_recv,
    pin_send, pin_recv, up_send, up_recv, down_send, down_recv,
    att_send, att_recv, cols_send, cols_recv, ret_send, ret_recv,
):
    z, x = lax.axis_index("ep_0"), lax.axis_index("ep_1")
    y, c = lax.axis_index("tp_0"), lax.axis_index("tp_1")
    ep, tp = z * X + x, y * C + c
    partner = {"tp_1": 1 - c}
    y_up, y_down = {"tp_0": lax.rem(y + 1, Y)}, {"tp_0": lax.rem(y + Y - 1, Y)}
    z_up, z_down = {"ep_0": lax.rem(z + 1, Z)}, {"ep_0": lax.rem(z + Z - 1, Z)}

    def ep_peer(distance):
        other = lax.rem(ep + distance, N_EP)
        return other, {"ep_0": other // X, "ep_1": lax.rem(other, X)}

    def tp_peer(distance):
        other = lax.rem(tp + distance, N_TP)
        return other, {"tp_0": other // C, "tp_1": lax.rem(other, C)}

    def x_peer(distance):
        return lax.rem(x + distance, X)

    def y_at(distance):
        return lax.rem(y + Y + distance, Y)

    def columns_of(other, width=COLS):
        return pl.ds(pl.multiple_of(other * width, width), width)

    def remote(src, dst, send_sem, recv_sem, device):
        return pltpu.make_async_remote_copy(
            src_ref=src, dst_ref=dst, send_sem=send_sem, recv_sem=recv_sem,
            device_id=device, device_id_type=MESH,
        )

    barrier = pltpu.get_barrier_semaphore()

    @pl.loop(1, N_EP)
    def _(distance):
        pl.semaphore_signal(barrier, 1, device_id=ep_peer(distance)[1], device_id_type=MESH)

    @pl.loop(1, N_TP)
    def _(distance):
        pl.semaphore_signal(barrier, 1, device_id=tp_peer(distance)[1], device_id_type=MESH)

    loads = {
        "route": (routes, route),
        "scale": (route_weight, route_scale),
        "tokens": (exp_rows, tokens),
        "token_gain": (exp_gain, token_gain),
        "gain_in": (mix_gain, gain_in),
        "rows": (mix_rows, rows),
        "query": (w_query, wqkv.at[pl.ds(0, HEAD)]),
        "key": (w_key, wqkv.at[pl.ds(2 * HEAD, HEAD)]),
        "value": (w_value, wqkv.at[pl.ds(3 * HEAD, HEAD)]),
        "w_out": (w_out, wo_own),
        "offset": (key_offset, offset),
        "gate": (w_gate.at[0], wgu.at[:, pl.ds(0, COLS)]),
        "up": (w_up.at[0], wgu.at[:, pl.ds(COLS, COLS)]),
        "down": (w_down.at[0], wd_own),
        "gain_out": (out_gain, gain_out),
    }
    loads = {
        name: pltpu.make_async_copy(a, b, load_sem.at[n])
        for n, (name, (a, b)) in enumerate(loads.items())
    }
    for load in loads.values():
        load.start()

    wqkv[pl.ds(HEAD, HEAD), :] = jnp.zeros((HEAD, D), BF16)
    tri[...] = jnp.where(
        (iota((256, 256), 1) >= HALF)
        | (lax.rem(iota((256, 256), 0), HALF) >= iota((256, 256), 1)), 1.0, 0.0,
    ).astype(BF16)

    for name in ("route", "scale", "tokens", "token_gain"):
        loads[name].wait()
    expert = iota((N_EP, TOK), 0)
    member = jnp.zeros((N_EP, TOK), F32)
    weight = jnp.zeros((N_EP, TOK), F32)
    for k in range(route.shape[0]):
        hit = route[k : k + 1, :] == expert
        member = member + jnp.where(hit, 1.0, 0.0)
        weight = weight + jnp.where(hit, route_scale[k : k + 1, :], 0.0)
    member = member.astype(BF16)
    earlier = jnp.where(iota((TOK, TOK), 0) < iota((TOK, TOK), 1), 1.0, 0.0).astype(BF16)
    before = dot(member, earlier).astype(BF16)
    spread = jnp.where(iota((SLOTS, N_EP), 0) // CAP == iota((SLOTS, N_EP), 1), 1.0, 0.0)
    spread = spread.astype(BF16)
    place = lax.rem(iota((SLOTS, TOK), 0), CAP).astype(F32)
    chosen = (dot(spread, member) > 0.5) & (dot(spread, before) == place)
    picks[...] = jnp.where(chosen, 1.0, 0.0).astype(BF16)
    high, low = split_two(weight)
    weight_hi[...] = jnp.where(chosen, dot(spread, high), 0.0).astype(BF16)
    weight_lo[...] = jnp.where(chosen, dot(spread, low), 0.0).astype(BF16)
    sent[...] = dot(picks[...], tokens[...]).astype(BF16)
    own_slots = pl.ds(pl.multiple_of(ep * CAP, CAP), CAP)
    grid[tp, own_slots, :] = sent[own_slots, :]
    gains[tp] = jnp.broadcast_to(token_gain[...], (GAIN_ROWS, COLS))

    loads["gain_in"].wait()
    loads["rows"].wait()
    gain = gain_in[...].astype(F32)
    gain = jnp.concatenate([gain[n : n + 1] for n in range(N_TP)], axis=1)

    @pl.loop(0, ROWS // 32)
    def _(n):
        at = pl.ds(pl.multiple_of(n * 32, 32), 32)
        numbers = rows[at, :].astype(F32)
        factor = lax.rsqrt(jnp.mean(numbers * numbers, axis=-1, keepdims=True) + EPSILON)
        rows[at, :] = (numbers * factor * gain).astype(BF16)

    for name in ("query", "key", "value"):
        loads[name].wait()
    projected = lax.dot_general(rows[...], wqkv[...], NT, preferred_element_type=F32).astype(BF16)
    q_pad[...] = projected[:, : 2 * HEAD]
    kvg[ep] = projected[:, 2 * HEAD :]
    loads["w_out"].wait()

    pl.semaphore_wait(barrier, N_EP - 1 + N_TP - 1)

    part_a, part_b = pl.ds(0, HALF), pl.ds(HALF, HALF)

    def send_a(slot, device):
        piece = kvg.at[slot, part_a]
        remote(piece, piece, kva_send, kva_recv.at[slot], device).start()

    def send_b(slot, device):
        piece = kvg.at[slot, part_b]
        remote(piece, piece, kvb_send, kvb_recv.at[slot], device).start()

    def wait_a(slot):
        piece = kvg.at[slot, part_a]
        remote(piece, piece, kva_send, kva_recv.at[slot], partner).wait_recv()

    def wait_b(slot):
        piece = kvg.at[slot, part_b]
        remote(piece, piece, kvb_send, kvb_recv.at[slot], partner).wait_recv()

    def send_b_across(slot):
        for distance in range(1, X):
            send_b(slot, {"ep_1": x_peer(distance)})

    @pl.loop(1, N_EP)
    def _(distance):
        other, device = ep_peer(distance)
        remote(
            sent.at[pl.ds(pl.multiple_of(other * CAP, CAP), CAP)],
            grid.at[tp, own_slots],
            disp_send, disp_recv, device,
        ).start()

    for distance in range(1, X):
        send_a(ep, {"ep_1": x_peer(distance)})
    send_b(ep, z_up)
    send_b(ep, z_down)
    send_a(ep, z_up)
    send_a(ep, z_down)
    send_b_across(ep)

    @pl.loop(1, N_TP)
    def _(distance):
        other, device = tp_peer(distance)
        remote(gains.at[tp], gains.at[tp], gain_send, gain_recv, device).start()
        remote(wo_own.at[:, columns_of(other)], wo.at[tp], wo_send, wo_recv, device).start()

    wo[tp] = wo_own[:, columns_of(tp)]

    for distance in range(1, X):
        slot = z * X + x_peer(distance)
        wait_a(slot)
        send_a(slot, z_up)
        send_a(slot, z_down)

    def attend(blocks, diagonal):
        count = len(blocks)
        scores = []
        for n, block in enumerate(blocks):
            shift = offset[:, pl.ds(pl.multiple_of(block * ROWS, ROWS), ROWS)] * LOG2E
            product = lax.dot_general(q_pad[...], kvg[block], NT, preferred_element_type=F32)
            product = product * (LOG2E / math.sqrt(HEAD)) + shift
            drop = jnp.maximum(jnp.log2(1.0 + jnp.exp2(jnp.minimum(product, 100.0))), product)
            if diagonal:
                visible = iota((ROWS, ROWS), 1) < iota((ROWS, ROWS), 0)
                drop = jnp.where(visible, drop, 0.0)
            scores.append(product)
            for half in range(2):
                high, low = split_two(drop[:, half * HALF : (half + 1) * HALF])
                at = pl.ds((2 * n + half) * ROWS, ROWS)
                drops[at, :HALF] = high
                drops[at, HALF:] = low
        totals = dot(drops[pl.ds(0, 2 * count * ROWS), :], tri[...])
        passed = jnp.zeros((ROWS, 128), F32)
        sums = jnp.zeros((ROWS, 128), F32)
        for n, block in enumerate(blocks):
            for half in (1, 0):
                at = slice(half * HALF, (half + 1) * HALF)
                total = totals[(2 * n + half) * ROWS : (2 * n + half + 1) * ROWS]
                weights = jnp.exp2(scores[n][:, at] - total[:, :HALF] - passed)
                if diagonal:
                    weights = jnp.where(visible[:, at], weights, 0.0)
                sums = sums + dot(weights.astype(BF16), kvg[block, pl.ds(half * HALF, HALF)])
                passed = passed + total[:, HALF:]
        return sums, passed

    def attend_near(blocks):
        sums, passed = attend(blocks, False)
        acc[...] += jnp.exp2(-carry[...]) * sums
        carry[...] += passed

    def row_blocks(row):
        return [row * X + X - 1 - n for n in range(X)]

    def near_row(back):
        @pl.when(z >= back)
        def _():
            attend_near(row_blocks(z - back))

    def far_row(back):
        @pl.when(z >= back)
        def _():
            sums, passed = attend(row_blocks(z - back), False)
            far[...] = sums + jnp.exp2(-passed) * far[...]

    def ring(buffer, pieces, send_sem, recv_sem):
        size = buffer.shape[1] // pieces
        early = pieces // 2

        def copy(slot, piece, device):
            block = buffer.at[slot, pl.ds(piece * size, size)]
            return remote(block, block, send_sem, recv_sem.at[slot, piece], device)

        def start():
            for piece in range(pieces):
                for device in (y_up, y_down, partner):
                    copy(tp, piece, device).start()

        def step(k):
            above, below = y_at(-k) * C + c, y_at(k) * C + c
            for piece in range(pieces):
                for slot, device, turn in ((above, y_up, True), (below, y_down, False)):
                    chosen = turn == (piece < early)
                    if k < Y // 2 or chosen:
                        copy(slot, piece, partner).wait_recv()
                        if k < Y // 2 - 1 or (k == Y // 2 - 1 and chosen):
                            copy(slot, piece, device).start()
                        copy(slot, piece, partner).start()

        def handed(chip):
            for piece in range(pieces):
                copy(chip * C + 1 - c, piece, partner).wait_recv()

        def drain():
            blocks = buffer.at[pl.ds(0, N_TP - 1)]
            remote(blocks, blocks, send_sem, recv_sem.at[0, 0], partner).wait_send()

        return start, step, handed, drain

    grid_start, grid_step, grid_handed, grid_drain = ring(grid, GRID_PIECES, grid_send, grid_recv)
    att_start, att_step, att_handed, att_drain = ring(att, ATT_PIECES, att_send, att_recv)
    cols_start, cols_step, cols_handed, cols_drain = ring(cols, COLS_PIECES, cols_send, cols_recv)

    arrived = grid.at[tp, pl.ds(0, SLOTS - CAP)]
    remote(arrived, arrived, disp_send, disp_recv, partner).wait_recv()
    grid_start()

    loads["offset"].wait()
    sums, passed = attend([ep], True)
    acc[...] = sums
    carry[...] = passed
    far[...] = jnp.zeros(far.shape, F32)
    for distance in range(1, X):
        wait_b(z * X + x_peer(distance))

    @pl.loop(0, x)
    def _(n):
        attend_near([ep - 1 - n])

    arrived = gains.at[pl.ds(0, N_TP - 1)]
    remote(arrived, arrived, gain_send, gain_recv, partner).wait_recv()
    loads["gate"].wait()
    loads["up"].wait()
    gu[...] = jnp.zeros(gu.shape, F32)
    ssq[...] = jnp.zeros(ssq.shape, F32)

    def gate_up(chip):
        scaled = []
        squares = ssq[...]
        for core in range(C):
            numbers = grid[chip * C + core].astype(F32)
            squares = squares + numbers * numbers
            scaled.append((numbers * gains[chip * C + core][:1].astype(F32)).astype(BF16))
        ssq[...] = squares
        gu[...] += dot(jnp.concatenate(scaled, axis=1), wgu[columns_of(chip, C * COLS), :])

    def kv_step(k):
        for distance in range(X):
            for row, device, turn in ((z + Z - k, z_up, True), (z + k, z_down, False)):
                slot = lax.rem(row, Z) * X + x_peer(distance)
                if k < Z // 2 or turn:
                    wait_a(slot)
                    if k < Z // 2 - 1 or (k == Z // 2 - 1 and turn):
                        send_a(slot, device)
        for row, device, turn in ((z + Z - k, z_up, True), (z + k, z_down, False)):
            slot = lax.rem(row, Z) * X + x
            if k < Z // 2 or turn:
                wait_b(slot)
                if k < Z // 2 - 1 or (k == Z // 2 - 1 and turn):
                    send_b(slot, device)
                send_b_across(slot)

    def kv_finish(row):
        for distance in range(1, X):
            wait_b(lax.rem(row, Z) * X + x_peer(distance))

    for k in range(1, 5):
        kv_step(k)
        grid_step(k)
        grid_handed(y_at(1 - k))
        gate_up(y_at(1 - k))
        if k > 1:
            grid_handed(y_at(k - 1))
            gate_up(y_at(k - 1))
            kv_finish(z + Z - k + 1)
            near_row(k - 1)
            kv_finish(z + k - 1)
            far_row(Z - k + 1)

    grid_handed(y_at(4))
    gate_up(y_at(4))
    factor = lax.rsqrt(jnp.sum(ssq[...], axis=1, keepdims=True) / D + EPSILON)
    gate_part = jnp.minimum(gu[:, :COLS] * factor, CLAMP_LIMIT)
    up_part = jnp.clip(gu[:, COLS:] * factor, -CLAMP_LIMIT, CLAMP_LIMIT)
    hidden = (up_part + 1.0) * (gate_part * jax.nn.sigmoid(SILU_SHARPNESS * gate_part))
    hidden = hidden.astype(BF16)
    loads["down"].wait()
    for distance in (4, -3, 3, -2, 2, -1, 1, 0):
        chip = y_at(distance)
        product = dot(hidden, wd_own[:, columns_of(chip, C * COLS)]).astype(BF16)
        for core in range(C):
            part[chip * C + core] = product[:, core * COLS : (core + 1) * COLS]
        remote(
            part.at[chip * C + 1 - c], pin.at[chip], pin_send, pin_recv.at[chip], partner
        ).start()

    kv_finish(z + Z - 4)
    near_row(4)
    acc[...] += jnp.exp2(-carry[...]) * far[...]
    first = pltpu.roll(acc[pl.ds(0, HALF), :], HEAD, 1)
    att[tp] = jnp.where(iota((HALF, 128), 1) < HEAD, first, acc[pl.ds(HALF, HALF), :]).astype(BF16)
    att_start()

    def own_sum(chip, piece):
        at = pl.ds(piece * SUM_ROWS, SUM_ROWS)
        return part[chip * C + c, at, :].astype(F32) + pin[chip, at, :].astype(F32)

    def wait_pin(chip):
        remote(part.at[chip], pin.at[chip], pin_send, pin_recv.at[chip], partner).wait_recv()

    ways = ((1, 4, y_up, up_out, up_in, up_send, up_recv), (-1, 3, y_down, down_out, down_in, down_send, down_recv))

    def sum_copy(way, hop, piece):
        _, _, device, out, into, send_sem, recv_sem = way
        at = pl.ds(piece * SUM_ROWS, SUM_ROWS)
        return remote(out.at[hop, at], into.at[hop, at], send_sem, recv_sem.at[hop, piece], device)

    def sum_step(hop):
        live = [way for way in ways if hop < way[1]]
        chips = [y_at(sign * (hops - hop)) for sign, hops, *_ in live]
        for chip in chips:
            wait_pin(chip)
        for piece in range(SUM_PIECES):
            at = pl.ds(piece * SUM_ROWS, SUM_ROWS)
            for way, chip in zip(live, chips):
                total = own_sum(chip, piece)
                if hop > 0:
                    sum_copy(way, hop - 1, piece).wait_recv()
                    total = total + way[4][hop - 1, at, :].astype(F32)
                way[3][hop, at, :] = total.astype(BF16)
                sum_copy(way, hop, piece).start()

    pieces = wo.at[pl.ds(0, N_TP - 1)]
    remote(pieces, pieces, wo_send, wo_recv, partner).wait_recv()
    for n in range(N_TP):
        zeros = jnp.zeros((HEAD, COLS), BF16)
        wo_wide[pl.ds(n * 128, HEAD), :] = jnp.concatenate([wo[n], zeros], axis=1)
        wo_wide[pl.ds(n * 128 + HEAD, HEAD), :] = jnp.concatenate([zeros, wo[n]], axis=1)

    for k in range(1, 5):
        sum_step(k - 1)
        att_step(k)
    for chip in range(Y):
        att_handed(chip)

    product = dot(jnp.concatenate([att[n] for n in range(N_TP)], axis=1), wo_wide[...])
    cols[tp, pl.ds(0, HALF), :] = product[:, :COLS].astype(BF16)
    cols[tp, pl.ds(HALF, HALF), :] = product[:, COLS:].astype(BF16)
    cols_start()

    wait_pin(y)
    for piece in range(SUM_PIECES):
        at = pl.ds(piece * SUM_ROWS, SUM_ROWS)
        total = own_sum(y, piece)
        for way in ways:
            sum_copy(way, way[1] - 1, piece).wait_recv()
            total = total + way[4][way[1] - 1, at, :].astype(F32)
        result[at, :] = total.astype(BF16)
    returned[own_slots, :] = result[own_slots, :]

    @pl.loop(1, N_EP)
    def _(distance):
        other, device = ep_peer(distance)
        remote(
            result.at[pl.ds(pl.multiple_of(other * CAP, CAP), CAP)],
            returned.at[own_slots],
            ret_send, ret_recv, device,
        ).start()

    for k in range(1, 5):
        cols_step(k)

    arrived = returned.at[pl.ds(0, SLOTS - CAP)]
    remote(arrived, arrived, ret_send, ret_recv, partner).wait_recv()
    total = lax.dot_general(weight_hi[...], returned[...], TN, preferred_element_type=F32)
    total += lax.dot_general(weight_lo[...], returned[...], TN, preferred_element_type=F32)
    exp_out[...] = total.astype(BF16)

    for chip in range(Y):
        cols_handed(chip)
    loads["gain_out"].wait()
    squares = jnp.zeros((ROWS, COLS), F32)
    for n in range(N_TP):
        numbers = cols[n].astype(F32)
        squares = squares + numbers * numbers
    factor = lax.rsqrt(jnp.sum(squares, axis=1, keepdims=True) / D + EPSILON)
    gain = gain_out[...].astype(F32)
    for n in range(N_TP):
        at = slice(n * COLS, (n + 1) * COLS)
        mix_out[:, at] = (cols[n].astype(F32) * factor * gain[n : n + 1]).astype(BF16)

    piece = kvg.at[pl.ds(0, N_EP - 1), part_a]
    remote(piece, piece, kva_send, kva_recv.at[0], partner).wait_send()
    remote(piece, piece, kvb_send, kvb_recv.at[0], partner).wait_send()
    piece = sent.at[pl.ds(0, SLOTS - CAP)]
    remote(piece, piece, disp_send, disp_recv, partner).wait_send()
    remote(piece, piece, ret_send, ret_recv, partner).wait_send()
    piece = gains.at[pl.ds(0, N_TP - 1)]
    remote(piece, piece, gain_send, gain_recv, partner).wait_send()
    piece = wo.at[pl.ds(0, N_TP - 1)]
    remote(piece, piece, wo_send, wo_recv, partner).wait_send()
    remote(pin, pin, pin_send, pin_recv.at[0], partner).wait_send()
    remote(up_in, up_in, up_send, up_recv.at[0, 0], partner).wait_send()
    remote(down_in, down_in, down_send, down_recv.at[0, 0], partner).wait_send()
    for drain in (grid_drain, att_drain, cols_drain):
        drain()


def on_device(*args):
    (mix_rows, mix_gain, w_query, w_key, w_value, key_offset, w_out, out_gain, exp_rows, exp_gain,
     routes, route_weight, w_gate, w_up, w_down) = args
    vmem, hbm = pl.BlockSpec(memory_space=pltpu.VMEM), pl.BlockSpec(memory_space=pl.ANY)
    dma = pltpu.SemaphoreType.DMA
    return pl.pallas_call(
        body,
        out_shape=(
            jax.ShapeDtypeStruct((ROWS, D), BF16),
            jax.ShapeDtypeStruct((TOK, COLS), BF16),
        ),
        in_specs=[hbm] * 15,
        out_specs=(vmem, vmem),
        scratch_shapes=[
            pltpu.VMEM((N_TP, COLS), BF16),
            pltpu.VMEM((N_TP, COLS), BF16),
            pltpu.VMEM((1, N_EP * ROWS), F32),
            pltpu.VMEM((TOK, COLS), BF16),
            pltpu.VMEM((1, COLS), BF16),
            pltpu.VMEM((4, TOK), jnp.int32),
            pltpu.VMEM((4, TOK), F32),
            pltpu.VMEM((ROWS, D), BF16),
            pltpu.VMEM((4 * HEAD, D), BF16),
            pltpu.VMEM((ROWS, 128), BF16),
            pltpu.VMEM((N_EP, ROWS, 128), BF16),
            pltpu.VMEM((ROWS, 128), F32),
            pltpu.VMEM((ROWS, 128), F32),
            pltpu.VMEM((ROWS, 128), F32),
            pltpu.VMEM((2 * X * ROWS, ROWS), BF16),
            pltpu.VMEM((256, 256), BF16),
            pltpu.VMEM((SLOTS, TOK), BF16),
            pltpu.VMEM((SLOTS, TOK), BF16),
            pltpu.VMEM((SLOTS, TOK), BF16),
            pltpu.VMEM((SLOTS, COLS), BF16),
            pltpu.VMEM((N_TP, SLOTS, COLS), BF16),
            pltpu.VMEM((N_TP, GAIN_ROWS, COLS), BF16),
            pltpu.VMEM((D, 2 * COLS), BF16),
            pltpu.VMEM((SLOTS, 2 * COLS), F32),
            pltpu.VMEM((SLOTS, COLS), F32),
            pltpu.VMEM((COLS, D), BF16),
            pltpu.VMEM((HEAD, D), BF16),
            pltpu.VMEM((N_TP, HEAD, COLS), BF16),
            pltpu.VMEM((N_TP * 128, 2 * COLS), BF16),
            pltpu.VMEM((N_TP, SLOTS, COLS), BF16),
            pltpu.VMEM((Y, SLOTS, COLS), BF16),
            pltpu.VMEM((4, SLOTS, COLS), BF16),
            pltpu.VMEM((4, SLOTS, COLS), BF16),
            pltpu.VMEM((3, SLOTS, COLS), BF16),
            pltpu.VMEM((3, SLOTS, COLS), BF16),
            pltpu.VMEM((N_TP, HALF, 128), BF16),
            pltpu.VMEM((N_TP, ROWS, COLS), BF16),
            pltpu.VMEM((SLOTS, COLS), BF16),
            pltpu.VMEM((SLOTS, COLS), BF16),
            dma((15,)),
            dma(()), dma(()),
            dma(()), dma((N_EP,)), dma(()), dma((N_EP,)),
            dma(()), dma((N_TP, GRID_PIECES)),
            dma(()), dma(()), dma(()), dma(()),
            dma(()), dma((Y,)),
            dma(()), dma((4, SUM_PIECES)), dma(()), dma((3, SUM_PIECES)),
            dma(()), dma((N_TP, ATT_PIECES)), dma(()), dma((N_TP, COLS_PIECES)),
            dma(()), dma(()),
        ],
        compiler_params=pltpu.CompilerParams(
            collective_id=0, has_side_effects=True, vmem_limit_bytes=60 * 1024 * 1024
        ),
    )(
        mix_rows, mix_gain.reshape(N_TP, COLS), w_query, w_key, w_value, key_offset, w_out,
        out_gain.reshape(N_TP, COLS), exp_rows, exp_gain.reshape(1, COLS), routes.T, route_weight.T,
        w_gate, w_up, w_down,
    )


def solution(mesh):
    torus = Mesh(mesh.devices.reshape(Z, X, Y, C), EP + TP)
    in_specs = (
        P(EP, None),
        P(),
        P(TP, None),
        P(TP, None),
        P(TP, None),
        P(TP, None),
        P(TP, None),
        P(),
        P(EP, TP),
        P(TP),
        P(EP, None),
        P(EP, None),
        P(EP, None, TP),
        P(EP, None, TP),
        P(EP, TP, None),
    )
    out_specs = (P(EP, None), P(EP, TP))
    return jax.shard_map(
        on_device, mesh=torus, in_specs=in_specs, out_specs=out_specs, check_vma=False
    )
```

time: 103 us -> 83.8 us (0.81)
  Pallas kernels: 95.8 us -> 80.1 us
  local copies, waits for them, and re-layouts: 6.34 us -> 2.92 us
    pallas_call x1, Pallas kernels: 95.8 us -> 80.1 us  [on_device(): pl.pallas_call(body, out_shape=(jax.ShapeDtypeStruct((ROWS, D), BF16), ja...]
    reshape x2 -> x0, local copies, waits for them, and re-layouts: 1.9 us -> none  [the longest x1 1.3 us: on_device(): mix_gain.reshape(1, D)]
    unnamed x12 -> x4, local copies, waits for them, and re-layouts: 4.45 us -> 2.92 us
where the time goes in v2:
time: 83.8 us; the launch traced here: 83.7 us
  Pallas kernels  80.1 us (96%)
  local copies, waits for them, and re-layouts  2.92 us (3%)
    pallas_call x1, Pallas kernels, on_device(): pl.pallas_call(body, out_shape=(jax.ShapeDtypeStruct((ROWS, D), BF16), ja...  80.1 us
    unnamed x4, local copies, waits for them, and re-layouts  2.92 us

profile of v2, /device:TPU:1, one launch (start us, length us, event | category | flops | bytes accessed | tf_op | source)
XLA Modules:
  0.0 83.7 jit_solution(10566621036706208187)
XLA Ops:
  0.6 80.1 %shard_map.158 = (bf16[256,2048]{1,0:T(8,128)(2,1)}, bf16[96,128]{1,0:T(8,128)(2,1)}) custom-call(bf16[256,2048]{1,0:T(8,128)(2,1)} %mix_rows.1, bf16[16,128]{1,0:T(8,128)(2,1)} %bitcast.5, bf16[64,2048]{1,0:T(8,128)(2,1)} %w_query.1, bf16[64,2048]{1,0:T(8,128)(2,1)} %w_key.1, bf16[64,2048]{1,0:T(8,128)(2,1)} %w_value.1, f32[1,8192]{1,0:T(1,128)} %key_offset.1, ...), custom_call_target="tpu_custom_call" | custom-call | tf_op jit(solution)/shard_map/pallas_call | solution.py:524
  80.8 0.0 copy-start
  80.8 2.3 %copy.19 = bf16[256,2048]{1,0:T(8,128)(2,1)} copy(bf16[256,2048]{1,0:T(8,128)(2,1)} %get-tuple-element.4) | data formatting | bytes 2097152
  83.1 0.0 copy-done
  83.1 0.6 copy.20
Async XLA Ops:
  80.8 2.3 %copy-start = (bf16[96,128]{1,0:T(8,128)(2,1)S(1)}, bf16[96,128]{1,0:T(8,128)(2,1)}, u32[]{:S(2)}) copy-start(bf16[96,128]{1,0:T(8,128)(2,1)} %get-tuple-element.5) | copy-start | bytes 73732

commit v3 on v2

v3 whole, which is shorter than its diff:
```python
import math

import jax
import jax.numpy as jnp
from jax import lax
from jax.experimental import pallas as pl
from jax.experimental.pallas import tpu as pltpu
from jax.sharding import Mesh
from jax.sharding import PartitionSpec as P

EP = ("ep_0", "ep_1")
TP = ("tp_0", "tp_1")
Z, X, Y, C = 8, 4, 8, 2
N_EP, N_TP = Z * X, Y * C

EPSILON = 1e-06
CLAMP_LIMIT = 7.0
SILU_SHARPNESS = 1.702
LOG2E = math.log2(math.e)

D = 2048
HEAD = 64
ROWS = 256
HALF = ROWS // 2
TOK = 96
CAP = 16
SLOTS = N_EP * CAP
COLS = D // N_TP
GAIN_ROWS = 16
GRID_PIECES, ATT_PIECES, SUM_PIECES = 4, 2, 4
SUM_ROWS = SLOTS // SUM_PIECES

F32 = jnp.float32
BF16 = jnp.bfloat16
MESH = pl.DeviceIdType.MESH
NT = (((1,), (1,)), ((), ()))
TN = (((0,), (0,)), ((), ()))


def dot(a, b):
    return jnp.dot(a, b, preferred_element_type=F32)


def iota(shape, dim):
    return lax.broadcasted_iota(jnp.int32, shape, dim)


def split_two(value):
    high = value.astype(BF16)
    return high, (value - high.astype(F32)).astype(BF16)


def body(
    mix_rows, mix_gain, w_query, w_key, w_value, key_offset, w_out, out_gain, exp_rows, exp_gain,
    routes, route_weight, w_gate, w_up, w_down,
    mix_out, exp_out,
    gain_in, gain_out, offset, tokens, token_gain, route, route_scale,
    rows, wqkv, q_pad, kvg, acc, carry, far, drops, tri,
    picks, weight_hi, weight_lo, sent, grid, gains, wgu, gu, ssq, wd_own, wo_own, wide, wide_other, mixed, mixed_out,
    part, pin, up_out, up_in, down_out, down_in,
    att, result, returned, exp_sum,
    load_sem, out_sem, disp_send, disp_recv, kva_send, kva_recv, kvb_send, kvb_recv, kvc_recv,
    wida_send, wida_recv, widb_send, widb_recv, widc_recv, over_send, over_recv,
    grid_send, grid_recv, grid_hand, gain_send, gain_recv, wo_send, wo_recv,
    pin_send, pin_recv, up_send, up_recv, down_send, down_recv,
    att_send, att_recv, att_hand, ret_send, ret_recv,
):
    z, x = lax.axis_index("ep_0"), lax.axis_index("ep_1")
    y, c = lax.axis_index("tp_0"), lax.axis_index("tp_1")
    ep, tp = z * X + x, y * C + c
    partner = {"tp_1": 1 - c}
    y_up, y_down = {"tp_0": lax.rem(y + 1, Y)}, {"tp_0": lax.rem(y + Y - 1, Y)}
    z_up, z_down = {"ep_0": lax.rem(z + 1, Z)}, {"ep_0": lax.rem(z + Z - 1, Z)}

    def ep_peer(turn):
        other = lax.rem(ep + 1 + lax.rem(turn + N_EP // 2 - 3, N_EP - 1), N_EP)
        return other, {"ep_0": other // X, "ep_1": lax.rem(other, X)}

    def tp_peer(distance):
        other = lax.rem(tp + distance, N_TP)
        return other, {"tp_0": other // C, "tp_1": lax.rem(other, C)}

    def x_peer(distance):
        return lax.rem(x + distance, X)

    def y_at(distance):
        return lax.rem(y + Y + distance, Y)

    def columns_of(other, width=COLS):
        return pl.ds(pl.multiple_of(other * width, width), width)

    def remote(src, dst, send_sem, recv_sem, device):
        return pltpu.make_async_remote_copy(
            src_ref=src, dst_ref=dst, send_sem=send_sem, recv_sem=recv_sem,
            device_id=device, device_id_type=MESH,
        )

    barrier = pltpu.get_barrier_semaphore()

    @pl.loop(1, N_EP)
    def _(distance):
        pl.semaphore_signal(barrier, 1, device_id=ep_peer(distance)[1], device_id_type=MESH)

    @pl.loop(1, N_TP)
    def _(distance):
        pl.semaphore_signal(barrier, 1, device_id=tp_peer(distance)[1], device_id_type=MESH)

    loads = {
        "route": (routes, route),
        "scale": (route_weight, route_scale),
        "tokens": (exp_rows, tokens),
        "token_gain": (exp_gain, token_gain),
        "gain_in": (mix_gain, gain_in),
        "rows": (mix_rows, rows),
        "query": (w_query, wqkv.at[pl.ds(0, HEAD)]),
        "key": (w_key, wqkv.at[pl.ds(2 * HEAD, HEAD)]),
        "value": (w_value, wqkv.at[pl.ds(3 * HEAD, HEAD)]),
        "w_out": (w_out, wo_own),
        "offset": (key_offset, offset),
        "gate": (w_gate.at[0], wgu.at[:, pl.ds(0, COLS)]),
        "up": (w_up.at[0], wgu.at[:, pl.ds(COLS, COLS)]),
        "down": (w_down.at[0], wd_own),
        "gain_out": (out_gain, gain_out),
    }
    loads = {
        name: pltpu.make_async_copy(a, b, load_sem.at[n])
        for n, (name, (a, b)) in enumerate(loads.items())
    }
    for load in loads.values():
        load.start()

    wqkv[pl.ds(HEAD, HEAD), :] = jnp.zeros((HEAD, D), BF16)
    later = lax.rem(iota((2 * ROWS, ROWS), 0), ROWS) >= iota((2 * ROWS, ROWS), 1)
    tri[...] = jnp.where(later, 1.0, 0.0).astype(BF16)

    for name in ("route", "scale", "tokens", "token_gain"):
        loads[name].wait()
    expert = iota((N_EP, TOK), 0)
    member = jnp.zeros((N_EP, TOK), F32)
    weight = jnp.zeros((N_EP, TOK), F32)
    for k in range(route.shape[0]):
        hit = route[k : k + 1, :] == expert
        member = member + jnp.where(hit, 1.0, 0.0)
        weight = weight + jnp.where(hit, route_scale[k : k + 1, :], 0.0)
    member = member.astype(BF16)
    earlier = jnp.where(iota((TOK, TOK), 0) < iota((TOK, TOK), 1), 1.0, 0.0).astype(BF16)
    before = dot(member, earlier).astype(BF16)
    spread = jnp.where(iota((SLOTS, N_EP), 0) // CAP == iota((SLOTS, N_EP), 1), 1.0, 0.0)
    spread = spread.astype(BF16)
    place = lax.rem(iota((SLOTS, TOK), 0), CAP).astype(F32)
    chosen = (dot(spread, member) > 0.5) & (dot(spread, before) == place)
    picks[...] = jnp.where(chosen, 1.0, 0.0).astype(BF16)
    high, low = split_two(weight)
    weight_hi[...] = jnp.where(chosen, dot(spread, high), 0.0).astype(BF16)
    weight_lo[...] = jnp.where(chosen, dot(spread, low), 0.0).astype(BF16)
    sent[...] = dot(picks[...], tokens[...]).astype(BF16)
    own_slots = pl.ds(pl.multiple_of(ep * CAP, CAP), CAP)
    grid[tp, own_slots, :] = sent[own_slots, :]
    gains[tp] = jnp.broadcast_to(token_gain[...], (GAIN_ROWS, COLS))

    pl.semaphore_wait(barrier, N_EP - 1 + N_TP - 1)

    @pl.loop(1, N_EP)
    def _(distance):
        other, device = ep_peer(distance)
        remote(
            sent.at[pl.ds(pl.multiple_of(other * CAP, CAP), CAP)],
            grid.at[tp, own_slots],
            disp_send, disp_recv, device,
        ).start()

    loads["w_out"].wait()
    wide_rows = pl.ds(pl.multiple_of((z // 2) * 16, 16), 16)
    wide_slots = pl.ds(pl.multiple_of(tp * 16, 16), 16)

    def wide_tile(core):
        group = x * 4 + core * 2 + lax.rem(z, 2)
        return wo_own.at[wide_rows, columns_of(group)]

    @pl.loop(1, N_TP)
    def _(distance):
        other, device = tp_peer(distance)
        remote(gains.at[tp], gains.at[tp], gain_send, gain_recv, device).start()
        remote(
            wide_tile(lax.rem(other, C)), wide.at[ep, wide_slots], wo_send, wo_recv, device
        ).start()

    wide[ep, wide_slots, :] = wide_tile(c)[...]

    loads["gain_in"].wait()
    loads["rows"].wait()
    gain = gain_in[...].astype(F32)
    gain = jnp.concatenate([gain[n : n + 1] for n in range(N_TP)], axis=1)

    @pl.loop(0, ROWS // 32)
    def _(n):
        at = pl.ds(pl.multiple_of(n * 32, 32), 32)
        numbers = rows[at, :].astype(F32)
        factor = lax.rsqrt(jnp.mean(numbers * numbers, axis=-1, keepdims=True) + EPSILON)
        rows[at, :] = (numbers * factor * gain).astype(BF16)

    for name in ("query", "key", "value"):
        loads[name].wait()
    projected = lax.dot_general(rows[...], wqkv[...], NT, preferred_element_type=F32).astype(BF16)
    q_pad[...] = projected[:, : 2 * HEAD]
    kvg[ep] = projected[:, 2 * HEAD :]

    def plane(buffer, a_send, a_recv, b_send, b_recv, c_recv):
        def copy_a(slot, device):
            piece = buffer.at[slot, pl.ds(0, HALF)]
            return remote(piece, piece, a_send, a_recv.at[slot], device)

        def copy_b(slot, device):
            piece = buffer.at[slot, pl.ds(HALF, HALF)]
            return remote(piece, piece, b_send, b_recv.at[slot // X], device)

        def b_across(slot):
            piece = buffer.at[slot, pl.ds(HALF, HALF)]
            for distance in range(1, X):
                device = {"ep_1": x_peer(distance)}
                remote(piece, piece, b_send, c_recv.at[slot // X], device).start()

        def start():
            for distance in range(1, X):
                copy_a(ep, {"ep_1": x_peer(distance)}).start()
            copy_b(ep, z_up).start()
            copy_b(ep, z_down).start()
            copy_a(ep, z_up).start()
            copy_a(ep, z_down).start()
            b_across(ep)

        def across():
            for distance in range(1, X):
                slot = z * X + x_peer(distance)
                copy_a(slot, partner).wait_recv()
                copy_a(slot, z_up).start()
                copy_a(slot, z_down).start()

        def step(k, distance):
            for row, device, turn in ((z + Z - k, z_up, True), (z + k, z_down, False)):
                slot = lax.rem(row, Z) * X + x_peer(distance)
                if k < Z // 2 or turn:
                    copy_a(slot, partner).wait_recv()
                    if k < Z // 2 - 1 or (k == Z // 2 - 1 and turn):
                        copy_a(slot, device).start()

        def step_b(k):
            for row, device, turn in ((z + Z - k, z_up, True), (z + k, z_down, False)):
                slot = lax.rem(row, Z) * X + x
                if k < Z // 2 or turn:
                    copy_b(slot, partner).wait_recv()
                    if k < Z // 2 - 1 or (k == Z // 2 - 1 and turn):
                        copy_b(slot, device).start()
                    b_across(slot)

        def finish(row):
            pieces = buffer.at[pl.ds(0, X - 1), pl.ds(HALF, HALF)]
            recv_sem = c_recv.at[lax.rem(row, Z)]
            remote(pieces, pieces, b_send, recv_sem, partner).wait_recv()

        def drain():
            piece = buffer.at[pl.ds(0, N_EP - 1), pl.ds(0, HALF)]
            remote(piece, piece, a_send, a_recv.at[0], partner).wait_send()
            remote(piece, piece, b_send, b_recv.at[0], partner).wait_send()

        return start, across, step, step_b, finish, drain

    kv_start, kv_across, kv_step, kv_step_b, kv_finish, kv_drain = plane(
        kvg, kva_send, kva_recv, kvb_send, kvb_recv, kvc_recv
    )
    wide_start, wide_across, wide_step, wide_step_b, wide_finish, wide_drain = plane(
        wide, wida_send, wida_recv, widb_send, widb_recv, widc_recv
    )

    kv_start()
    def attend(blocks, diagonal):
        count = len(blocks)
        scores = []
        for n, block in enumerate(blocks):
            shift = offset[:, pl.ds(pl.multiple_of(block * ROWS, ROWS), ROWS)] * LOG2E
            product = lax.dot_general(q_pad[...], kvg[block], NT, preferred_element_type=F32)
            product = product * (LOG2E / math.sqrt(HEAD)) + shift
            drop = jnp.maximum(LOG2E * jnp.log(1.0 + jnp.exp2(jnp.minimum(product, 100.0))), product)
            if diagonal:
                visible = iota((ROWS, ROWS), 1) < iota((ROWS, ROWS), 0)
                drop = jnp.where(visible, drop, 0.0)
            scores.append(product)
            high, low = split_two(drop)
            at = pl.ds(n * ROWS, ROWS)
            drops[at, :ROWS] = high
            drops[at, ROWS:] = low
        passed = jnp.zeros((ROWS, 1), F32)
        sums = jnp.zeros((ROWS, 128), F32)
        totals = dot(drops[pl.ds(0, count * ROWS), :], tri[...])
        for n, block in enumerate(blocks):
            total = totals[n * ROWS : (n + 1) * ROWS]
            weights = jnp.exp2(scores[n] - (total + passed))
            if diagonal:
                weights = jnp.where(visible, weights, 0.0)
            sums = sums + dot(weights.astype(BF16), kvg[block])
            passed = passed + total[:, :1]
        return sums, passed

    def attend_near(blocks):
        sums, passed = attend(blocks, False)
        acc[...] += jnp.exp2(-carry[...]) * sums
        carry[...] += passed

    def row_blocks(row):
        return [row * X + X - 1 - n for n in range(X)]

    def near_row(back):
        @pl.when(z >= back)
        def _():
            attend_near(row_blocks(z - back))

    def far_row(back):
        @pl.when(z >= back)
        def _():
            sums, passed = attend(row_blocks(z - back), False)
            far[...] = sums + jnp.exp2(-passed) * far[...]

    def ring(buffer, pieces, send_sem, recv_sem, hand_sem):
        size = buffer.shape[1] // pieces
        early = pieces // 2

        def copy(slot, piece, device):
            block = buffer.at[slot, pl.ds(piece * size, size)]
            return remote(block, block, send_sem, recv_sem.at[slot // C, piece], device)

        def hand(slot, piece):
            block = buffer.at[slot, pl.ds(piece * size, size)]
            remote(block, block, send_sem, hand_sem.at[slot // C], partner).start()

        def start():
            for piece in range(pieces):
                copy(tp, piece, y_up).start()
                copy(tp, piece, y_down).start()
                hand(tp, piece)

        def step(k, piece):
            above, below = y_at(-k) * C + c, y_at(k) * C + c
            for slot, device, turn in ((above, y_up, True), (below, y_down, False)):
                chosen = turn == (piece < early)
                if k < Y // 2 or chosen:
                    copy(slot, piece, partner).wait_recv()
                    if k < Y // 2 - 1 or (k == Y // 2 - 1 and chosen):
                        copy(slot, piece, device).start()
                    hand(slot, piece)

        def handed(chip):
            block = buffer.at[chip * C + 1 - c]
            remote(block, block, send_sem, hand_sem.at[chip], partner).wait_recv()

        def drain():
            blocks = buffer.at[pl.ds(0, N_TP - 1)]
            remote(blocks, blocks, send_sem, hand_sem.at[0], partner).wait_send()

        return start, step, handed, drain

    grid_start, grid_step, grid_handed, grid_drain = ring(
        grid, GRID_PIECES, grid_send, grid_recv, grid_hand
    )
    att_start, att_step, att_handed, att_drain = ring(
        att, ATT_PIECES, att_send, att_recv, att_hand
    )

    arrived = grid.at[tp, pl.ds(0, SLOTS - CAP)]
    remote(arrived, arrived, disp_send, disp_recv, partner).wait_recv()
    grid_start()
    kv_across()
    loads["offset"].wait()
    sums, passed = attend([ep], True)
    acc[...] = sums
    carry[...] = jnp.broadcast_to(passed, carry.shape)
    far[...] = jnp.zeros(far.shape, F32)
    kv_finish(z)

    @pl.loop(0, x)
    def _(n):
        attend_near([ep - 1 - n])

    arrived = gains.at[pl.ds(0, N_TP - 1)]
    remote(arrived, arrived, gain_send, gain_recv, partner).wait_recv()
    loads["gate"].wait()
    loads["up"].wait()
    gu[...] = jnp.zeros(gu.shape, F32)
    ssq[...] = jnp.zeros(ssq.shape, F32)

    def gate_up(chip):
        scaled = []
        squares = ssq[...]
        for core in range(C):
            numbers = grid[chip * C + core].astype(F32)
            squares = squares + numbers * numbers
            scaled.append((numbers * gains[chip * C + core][:1].astype(F32)).astype(BF16))
        ssq[...] = squares
        gu[...] += dot(jnp.concatenate(scaled, axis=1), wgu[columns_of(chip, C * COLS), :])

    for k in range(1, 5):
        for piece in range(GRID_PIECES):
            grid_step(k, piece)
            kv_step(k, piece)
        kv_step_b(k)
        grid_handed(y_at(1 - k))
        gate_up(y_at(1 - k))
        if k > 1:
            grid_handed(y_at(k - 1))
            gate_up(y_at(k - 1))
        if k == 2:
            kv_finish(z + Z - 1)
            near_row(1)
        if k == 3:
            kv_finish(z + Z - 2)
            near_row(2)
            kv_finish(z + 1)
            far_row(7)

    pieces = wide.at[ep, pl.ds(0, ROWS - 16)]
    remote(pieces, pieces, wo_send, wo_recv, partner).wait_recv()
    wide_start()
    grid_handed(y_at(4))
    gate_up(y_at(4))
    factor = lax.rsqrt(jnp.sum(ssq[...], axis=1, keepdims=True) / D + EPSILON)
    gate_part = jnp.minimum(gu[:, :COLS] * factor, CLAMP_LIMIT)
    up_part = jnp.clip(gu[:, COLS:] * factor, -CLAMP_LIMIT, CLAMP_LIMIT)
    hidden = (up_part + 1.0) * (gate_part * jax.nn.sigmoid(SILU_SHARPNESS * gate_part))
    hidden = hidden.astype(BF16)
    loads["down"].wait()
    def down(distance):
        chip = y_at(distance)
        product = dot(hidden, wd_own[:, columns_of(chip, C * COLS)]).astype(BF16)
        for core in range(C):
            part[chip * C + core] = product[:, core * COLS : (core + 1) * COLS]
        remote(
            part.at[chip * C + 1 - c], pin.at[chip], pin_send, pin_recv.at[chip], partner
        ).start()

    for distance in (4, 3, -3):
        down(distance)

    def own_sum(chip, piece):
        at = pl.ds(piece * SUM_ROWS, SUM_ROWS)
        return part[chip * C + c, at, :].astype(F32) + pin[chip, at, :].astype(F32)

    def wait_pin(chip):
        remote(part.at[chip], pin.at[chip], pin_send, pin_recv.at[chip], partner).wait_recv()

    ways = (
        (1, True, y_up, up_out, up_in, up_send, up_recv),
        (-1, False, y_down, down_out, down_in, down_send, down_recv),
    )
    seen = set()

    def hops_of(way, piece):
        return 4 if way[1] == (piece < SUM_PIECES // 2) else 3

    def sum_copy(way, hop, piece):
        _, _, device, out, into, send_sem, recv_sem = way
        at = pl.ds(piece * SUM_ROWS, SUM_ROWS)
        return remote(out.at[hop, at], into.at[hop, at], send_sem, recv_sem.at[hop, piece], device)

    def sum_step(hop, piece):
        at = pl.ds(piece * SUM_ROWS, SUM_ROWS)
        for way in ways:
            distance = hops_of(way, piece) - hop
            if distance > 0:
                distance = way[0] * distance if distance < 4 else 4
                if distance not in seen:
                    seen.add(distance)
                    wait_pin(y_at(distance))
                total = own_sum(y_at(distance), piece)
                if hop > 0:
                    sum_copy(way, hop - 1, piece).wait_recv()
                    total = total + way[4][hop - 1, at, :].astype(F32)
                way[3][hop, at, :] = total.astype(BF16)
                sum_copy(way, hop, piece).start()

    for piece in range(SUM_PIECES):
        sum_step(0, piece)
    wide_across()
    for distance in (2, -2, 1, -1, 0):
        down(distance)
    kv_finish(z + Z - 3)
    near_row(3)
    kv_finish(z + 2)
    far_row(6)

    def hand_over(row):
        wide_finish(row)
        block = pl.ds(pl.multiple_of(lax.rem(row, Z) * X, X), X)
        at = lax.rem(row, Z)
        remote(wide.at[block], wide_other.at[block], over_send, over_recv.at[at], partner).start()

    for piece in range(SUM_PIECES):
        sum_step(1, piece)
        wide_step(1, piece)
    wide_step_b(1)
    hand_over(z)
    kv_finish(z + 3)
    far_row(5)
    kv_finish(z + Z - 4)
    near_row(4)
    acc[...] += jnp.exp2(-carry[...]) * far[...]
    att[tp] = jnp.transpose(acc[...])[HEAD:].astype(BF16)
    att_start()
    for piece in range(SUM_PIECES):
        sum_step(2, piece)
        wide_step(2, piece)
    wide_step_b(2)
    hand_over(z + Z - 1)
    hand_over(z + 1)
    for piece in range(ATT_PIECES):
        att_step(1, piece)
    for piece in range(SUM_PIECES):
        sum_step(3, piece)
        wide_step(3, piece)
    wide_step_b(3)
    hand_over(z + Z - 2)
    hand_over(z + 2)
    for piece in range(ATT_PIECES):
        att_step(2, piece)
    wait_pin(y)
    for piece in range(SUM_PIECES):
        at = pl.ds(piece * SUM_ROWS, SUM_ROWS)
        total = own_sum(y, piece)
        for way in ways:
            hop = hops_of(way, piece) - 1
            sum_copy(way, hop, piece).wait_recv()
            total = total + way[4][hop, at, :].astype(F32)
        result[at, :] = total.astype(BF16)
    returned[own_slots, :] = result[own_slots, :]

    @pl.loop(1, N_EP)
    def _(distance):
        other, device = ep_peer(distance)
        remote(
            result.at[pl.ds(pl.multiple_of(other * CAP, CAP), CAP)],
            returned.at[own_slots],
            ret_send, ret_recv, device,
        ).start()

    for piece in range(X):
        wide_step(4, piece)
    wide_step_b(4)
    for piece in range(ATT_PIECES):
        att_step(3, piece)
    hand_over(z + Z - 3)
    hand_over(z + 3)
    for piece in range(ATT_PIECES):
        att_step(4, piece)
    hand_over(z + 4)
    for chip in range(Y):
        att_handed(chip)
    for row in range(Z):
        block = wide.at[pl.ds(row * X, X)]
        remote(block, block, over_send, over_recv.at[row], partner).wait_recv()

    left = jnp.concatenate(
        [att[:, pl.ds(16 * n, 16), :].reshape(ROWS, ROWS) for n in range(4)], axis=0
    )
    left = jnp.transpose(left)
    squares = jnp.zeros((ROWS, COLS), F32)

    def project_out(core, source):
        squares = jnp.zeros((ROWS, COLS), F32)
        for across in range(X):
            right = jnp.concatenate(
                [
                    jnp.concatenate([source[(2 * n + m) * X + across] for n in range(4)], axis=0)
                    for m in range(2)
                ],
                axis=1,
            )
            product = dot(left, right)
            mixed[:, columns_of(across * 2 + core, 2 * COLS)] = product
            for m in range(2):
                numbers = product[:, m * COLS : (m + 1) * COLS]
                squares = squares + numbers * numbers
        return squares

    squares = project_out(c, wide) + project_out(1 - c, wide_other)
    loads["gain_out"].wait()
    factor = lax.rsqrt(jnp.sum(squares, axis=1, keepdims=True) / D + EPSILON)
    gain = gain_out[...].astype(F32)
    mix_copies = []
    for n in range(N_TP):
        at = pl.ds(n * COLS, COLS)
        mixed_out[:, at] = (mixed[:, at] * factor * gain[n : n + 1]).astype(BF16)
        if n % 4 == 3:
            at = pl.ds((n - 3) * COLS, 4 * COLS)
            mix_copies.append(
                pltpu.make_async_copy(mixed_out.at[:, at], mix_out.at[:, at], out_sem.at[n // 4])
            )
            mix_copies[-1].start()

    arrived = returned.at[pl.ds(0, SLOTS - CAP)]
    remote(arrived, arrived, ret_send, ret_recv, partner).wait_recv()
    total = lax.dot_general(weight_hi[...], returned[...], TN, preferred_element_type=F32)
    total += lax.dot_general(weight_lo[...], returned[...], TN, preferred_element_type=F32)
    exp_sum[...] = total.astype(BF16)
    exp_copy = pltpu.make_async_copy(exp_sum, exp_out, out_sem.at[4])
    exp_copy.start()

    kv_drain()
    wide_drain()
    remote(wide, wide, over_send, over_recv.at[0], partner).wait_send()
    piece = sent.at[pl.ds(0, SLOTS - CAP)]
    remote(piece, piece, disp_send, disp_recv, partner).wait_send()
    remote(piece, piece, ret_send, ret_recv, partner).wait_send()
    piece = gains.at[pl.ds(0, N_TP - 1)]
    remote(piece, piece, gain_send, gain_recv, partner).wait_send()
    piece = wide.at[0, pl.ds(0, ROWS - 16)]
    remote(piece, piece, wo_send, wo_recv, partner).wait_send()
    remote(pin, pin, pin_send, pin_recv.at[0], partner).wait_send()
    for into, send_sem, recv_sem in ((up_in, up_send, up_recv), (down_in, down_send, down_recv)):
        for piece in (into.at[pl.ds(0, 3)], into.at[3, pl.ds(0, SLOTS // 2)]):
            remote(piece, piece, send_sem, recv_sem.at[0, 0], partner).wait_send()
    grid_drain()
    att_drain()
    for copy in (*mix_copies, exp_copy):
        copy.wait()


def on_device(*args):
    (mix_rows, mix_gain, w_query, w_key, w_value, key_offset, w_out, out_gain, exp_rows, exp_gain,
     routes, route_weight, w_gate, w_up, w_down) = args
    hbm = pl.BlockSpec(memory_space=pl.ANY)
    dma = pltpu.SemaphoreType.DMA
    return pl.pallas_call(
        body,
        out_shape=(
            jax.ShapeDtypeStruct((ROWS, D), BF16),
            jax.ShapeDtypeStruct((TOK, COLS), BF16),
        ),
        in_specs=[hbm] * 15,
        out_specs=(hbm, hbm),
        scratch_shapes=[
            pltpu.VMEM((N_TP, COLS), BF16),
            pltpu.VMEM((N_TP, COLS), BF16),
            pltpu.VMEM((1, N_EP * ROWS), F32),
            pltpu.VMEM((TOK, COLS), BF16),
            pltpu.VMEM((1, COLS), BF16),
            pltpu.VMEM((4, TOK), jnp.int32),
            pltpu.VMEM((4, TOK), F32),
            pltpu.VMEM((ROWS, D), BF16),
            pltpu.VMEM((4 * HEAD, D), BF16),
            pltpu.VMEM((ROWS, 128), BF16),
            pltpu.VMEM((N_EP, ROWS, 128), BF16),
            pltpu.VMEM((ROWS, 128), F32),
            pltpu.VMEM((ROWS, 128), F32),
            pltpu.VMEM((ROWS, 128), F32),
            pltpu.VMEM((X * ROWS, 2 * ROWS), BF16),
            pltpu.VMEM((2 * ROWS, ROWS), BF16),
            pltpu.VMEM((SLOTS, TOK), BF16),
            pltpu.VMEM((SLOTS, TOK), BF16),
            pltpu.VMEM((SLOTS, TOK), BF16),
            pltpu.VMEM((SLOTS, COLS), BF16),
            pltpu.VMEM((N_TP, SLOTS, COLS), BF16),
            pltpu.VMEM((N_TP, GAIN_ROWS, COLS), BF16),
            pltpu.VMEM((D, 2 * COLS), BF16),
            pltpu.VMEM((SLOTS, 2 * COLS), F32),
            pltpu.VMEM((SLOTS, COLS), F32),
            pltpu.VMEM((COLS, D), BF16),
            pltpu.VMEM((HEAD, D), BF16),
            pltpu.VMEM((N_EP, ROWS, 128), BF16),
            pltpu.VMEM((N_EP, ROWS, 128), BF16),
            pltpu.VMEM((ROWS, D), F32),
            pltpu.VMEM((ROWS, D), BF16),
            pltpu.VMEM((N_TP, SLOTS, COLS), BF16),
            pltpu.VMEM((Y, SLOTS, COLS), BF16),
            pltpu.VMEM((4, SLOTS, COLS), BF16),
            pltpu.VMEM((4, SLOTS, COLS), BF16),
            pltpu.VMEM((4, SLOTS, COLS), BF16),
            pltpu.VMEM((4, SLOTS, COLS), BF16),
            pltpu.VMEM((N_TP, HEAD, ROWS), BF16),
            pltpu.VMEM((SLOTS, COLS), BF16),
            pltpu.VMEM((SLOTS, COLS), BF16),
            pltpu.VMEM((TOK, COLS), BF16),
            dma((15,)), dma((5,)),
            dma(()), dma(()),
            dma(()), dma((N_EP,)), dma(()), dma((Z,)), dma((Z,)),
            dma(()), dma((N_EP,)), dma(()), dma((Z,)), dma((Z,)),
            dma(()), dma((Z,)),
            dma(()), dma((Y, GRID_PIECES)), dma((Y,)),
            dma(()), dma(()), dma(()), dma(()),
            dma(()), dma((Y,)),
            dma(()), dma((4, SUM_PIECES)), dma(()), dma((4, SUM_PIECES)),
            dma(()), dma((Y, ATT_PIECES)), dma((Y,)),
            dma(()), dma(()),
        ],
        compiler_params=pltpu.CompilerParams(
            collective_id=0, has_side_effects=True, vmem_limit_bytes=60 * 1024 * 1024
        ),
    )(
        mix_rows, mix_gain.reshape(N_TP, COLS), w_query, w_key, w_value, key_offset, w_out,
        out_gain.reshape(N_TP, COLS), exp_rows, exp_gain.reshape(1, COLS), routes.T, route_weight.T,
        w_gate, w_up, w_down,
    )


def solution(mesh):
    torus = Mesh(mesh.devices.reshape(Z, X, Y, C), EP + TP)
    in_specs = (
        P(EP, None),
        P(),
        P(TP, None),
        P(TP, None),
        P(TP, None),
        P(TP, None),
        P(TP, None),
        P(),
        P(EP, TP),
        P(TP),
        P(EP, None),
        P(EP, None),
        P(EP, None, TP),
        P(EP, None, TP),
        P(EP, TP, None),
    )
    out_specs = (P(EP, None), P(EP, TP))
    return jax.shard_map(
        on_device, mesh=torus, in_specs=in_specs, out_specs=out_specs, check_vma=False
    )
```

time: 83.8 us -> 77.2 us (0.921)
  Pallas kernels: 80.1 us -> 73.5 us
    pallas_call x1, Pallas kernels: 80.1 us -> 73.5 us  [on_device(): pl.pallas_call(body, out_shape=(jax.ShapeDtypeStruct((ROWS, D), BF16), ja...]
where the time goes in v3:
time: 77.2 us; the launch traced here: 77.1 us
  Pallas kernels  73.5 us (95%)
  local copies, waits for them, and re-layouts  2.92 us (4%)
    pallas_call x1, Pallas kernels, on_device(): pl.pallas_call(body, out_shape=(jax.ShapeDtypeStruct((ROWS, D), BF16), ja...  73.5 us
    unnamed x4, local copies, waits for them, and re-layouts  2.92 us

profile of v3, /device:TPU:1, one launch (start us, length us, event | category | flops | bytes accessed | tf_op | source)
XLA Modules:
  0.0 77.1 jit_solution(10534816047622543566)
XLA Ops:
  0.6 73.5 %shard_map.158 = (bf16[256,2048]{1,0:T(8,128)(2,1)}, bf16[96,128]{1,0:T(8,128)(2,1)}) custom-call(bf16[256,2048]{1,0:T(8,128)(2,1)} %mix_rows.1, bf16[16,128]{1,0:T(8,128)(2,1)} %bitcast.5, bf16[64,2048]{1,0:T(8,128)(2,1)} %w_query.1, bf16[64,2048]{1,0:T(8,128)(2,1)} %w_key.1, bf16[64,2048]{1,0:T(8,128)(2,1)} %w_value.1, f32[1,8192]{1,0:T(1,128)} %key_offset.1, ...), custom_call_target="tpu_custom_call" | custom-call | tf_op jit(solution)/shard_map/pallas_call | solution.py:630
  74.1 0.0 copy-start
  74.1 2.3 %copy.19 = bf16[256,2048]{1,0:T(8,128)(2,1)} copy(bf16[256,2048]{1,0:T(8,128)(2,1)} %get-tuple-element.4) | data formatting | bytes 2097152
  76.5 0.0 copy-done
  76.5 0.6 copy.20
Async XLA Ops:
  74.1 2.3 %copy-start = (bf16[96,128]{1,0:T(8,128)(2,1)S(1)}, bf16[96,128]{1,0:T(8,128)(2,1)}, u32[]{:S(2)}) copy-start(bf16[96,128]{1,0:T(8,128)(2,1)} %get-tuple-element.5) | copy-start | bytes 73732

commit v4 on v3

--- a/solution.py
+++ b/solution.py
@@ -27,7 +27,7 @@
 SLOTS = N_EP * CAP
 COLS = D // N_TP
 GAIN_ROWS = 16
-GRID_PIECES, ATT_PIECES, SUM_PIECES = 4, 2, 4
+GRID_PIECES, SUM_PIECES = 4, 4
 SUM_ROWS = SLOTS // SUM_PIECES
 
 F32 = jnp.float32
@@ -55,7 +55,7 @@
     routes, route_weight, w_gate, w_up, w_down,
     mix_out, exp_out,
     gain_in, gain_out, offset, tokens, token_gain, route, route_scale,
-    rows, wqkv, q_pad, kvg, acc, carry, far, drops, tri,
+    rows, wqkv, q_pad, q_help, kvg, acc, carry, far, far_out, far_in, drops, tri,
     picks, weight_hi, weight_lo, sent, grid, gains, wgu, gu, ssq, wd_own, wo_own, wide, wide_other, mixed, mixed_out,
     part, pin, up_out, up_in, down_out, down_in,
     att, result, returned, exp_sum,
@@ -63,7 +63,8 @@
     wida_send, wida_recv, widb_send, widb_recv, widc_recv, over_send, over_recv,
     grid_send, grid_recv, grid_hand, gain_send, gain_recv, wo_send, wo_recv,
     pin_send, pin_recv, up_send, up_recv, down_send, down_recv,
-    att_send, att_recv, att_hand, ret_send, ret_recv,
+    att_send, att_recv, att_other, ret_send, ret_recv,
+    q_send, q_recv, far_send, far_recv,
 ):
     z, x = lax.axis_index("ep_0"), lax.axis_index("ep_1")
     y, c = lax.axis_index("tp_0"), lax.axis_index("tp_1")
@@ -97,11 +98,11 @@
 
     barrier = pltpu.get_barrier_semaphore()
 
-    @pl.loop(1, N_EP)
+    @pl.loop(1, N_EP, unroll=True)
     def _(distance):
         pl.semaphore_signal(barrier, 1, device_id=ep_peer(distance)[1], device_id_type=MESH)
 
-    @pl.loop(1, N_TP)
+    @pl.loop(1, N_TP, unroll=True)
     def _(distance):
         pl.semaphore_signal(barrier, 1, device_id=tp_peer(distance)[1], device_id_type=MESH)
 
@@ -130,8 +131,7 @@
         load.start()
 
     wqkv[pl.ds(HEAD, HEAD), :] = jnp.zeros((HEAD, D), BF16)
-    later = lax.rem(iota((2 * ROWS, ROWS), 0), ROWS) >= iota((2 * ROWS, ROWS), 1)
-    tri[...] = jnp.where(later, 1.0, 0.0).astype(BF16)
+    tri[...] = jnp.where(iota((ROWS, ROWS), 0) > iota((ROWS, ROWS), 1), 1.0, 0.0).astype(BF16)
 
     for name in ("route", "scale", "tokens", "token_gain"):
         loads[name].wait()
@@ -158,9 +158,27 @@
     grid[tp, own_slots, :] = sent[own_slots, :]
     gains[tp] = jnp.broadcast_to(token_gain[...], (GAIN_ROWS, COLS))
 
+    loads["gain_in"].wait()
+    loads["rows"].wait()
+    gain = gain_in[...].astype(F32)
+    gain = jnp.concatenate([gain[n : n + 1] for n in range(N_TP)], axis=1)
+
+    @pl.loop(0, ROWS // 32)
+    def _(n):
+        at = pl.ds(pl.multiple_of(n * 32, 32), 32)
+        numbers = rows[at, :].astype(F32)
+        factor = lax.rsqrt(jnp.mean(numbers * numbers, axis=-1, keepdims=True) + EPSILON)
+        rows[at, :] = (numbers * factor * gain).astype(BF16)
+
+    for name in ("query", "key", "value"):
+        loads[name].wait()
+    projected = lax.dot_general(rows[...], wqkv[...], NT, preferred_element_type=F32).astype(BF16)
+    q_pad[...] = projected[:, : 2 * HEAD]
+    kvg[ep] = projected[:, 2 * HEAD :]
+
     pl.semaphore_wait(barrier, N_EP - 1 + N_TP - 1)
 
-    @pl.loop(1, N_EP)
+    @pl.loop(1, N_EP, unroll=True)
     def _(distance):
         other, device = ep_peer(distance)
         remote(
@@ -168,42 +186,6 @@
             grid.at[tp, own_slots],
             disp_send, disp_recv, device,
         ).start()
-
-    loads["w_out"].wait()
-    wide_rows = pl.ds(pl.multiple_of((z // 2) * 16, 16), 16)
-    wide_slots = pl.ds(pl.multiple_of(tp * 16, 16), 16)
-
-    def wide_tile(core):
-        group = x * 4 + core * 2 + lax.rem(z, 2)
-        return wo_own.at[wide_rows, columns_of(group)]
-
-    @pl.loop(1, N_TP)
-    def _(distance):
-        other, device = tp_peer(distance)
-        remote(gains.at[tp], gains.at[tp], gain_send, gain_recv, device).start()
-        remote(
-            wide_tile(lax.rem(other, C)), wide.at[ep, wide_slots], wo_send, wo_recv, device
-        ).start()
-
-    wide[ep, wide_slots, :] = wide_tile(c)[...]
-
-    loads["gain_in"].wait()
-    loads["rows"].wait()
-    gain = gain_in[...].astype(F32)
-    gain = jnp.concatenate([gain[n : n + 1] for n in range(N_TP)], axis=1)
-
-    @pl.loop(0, ROWS // 32)
-    def _(n):
-        at = pl.ds(pl.multiple_of(n * 32, 32), 32)
-        numbers = rows[at, :].astype(F32)
-        factor = lax.rsqrt(jnp.mean(numbers * numbers, axis=-1, keepdims=True) + EPSILON)
-        rows[at, :] = (numbers * factor * gain).astype(BF16)
-
-    for name in ("query", "key", "value"):
-        loads[name].wait()
-    projected = lax.dot_general(rows[...], wqkv[...], NT, preferred_element_type=F32).astype(BF16)
-    q_pad[...] = projected[:, : 2 * HEAD]
-    kvg[ep] = projected[:, 2 * HEAD :]
 
     def plane(buffer, a_send, a_recv, b_send, b_recv, c_recv):
         def copy_a(slot, device):
@@ -273,36 +255,59 @@
     )
 
     kv_start()
-    def attend(blocks, diagonal):
+    across_z = {"ep_0": Z - 1 - z}
+
+    @pl.when(z >= 5)
+    def _():
+        remote(q_pad, q_help, q_send, q_recv, across_z).start()
+
+    loads["w_out"].wait()
+    wide_rows = pl.ds(pl.multiple_of((z // 2) * 16, 16), 16)
+    wide_slots = pl.ds(pl.multiple_of(tp * 16, 16), 16)
+
+    def wide_tile(core):
+        group = x * 4 + core * 2 + lax.rem(z, 2)
+        return wo_own.at[wide_rows, columns_of(group)]
+
+    @pl.loop(1, N_TP, unroll=True)
+    def _(distance):
+        other, device = tp_peer(distance)
+        remote(gains.at[tp], gains.at[tp], gain_send, gain_recv, device).start()
+        remote(
+            wide_tile(lax.rem(other, C)), wide.at[ep, wide_slots], wo_send, wo_recv, device
+        ).start()
+
+    wide[ep, wide_slots, :] = wide_tile(c)[...]
+
+    def attend(blocks, diagonal=False, query=q_pad):
         count = len(blocks)
-        scores = []
+        takes, firsts = [], []
         for n, block in enumerate(blocks):
             shift = offset[:, pl.ds(pl.multiple_of(block * ROWS, ROWS), ROWS)] * LOG2E
-            product = lax.dot_general(q_pad[...], kvg[block], NT, preferred_element_type=F32)
-            product = product * (LOG2E / math.sqrt(HEAD)) + shift
-            drop = jnp.maximum(LOG2E * jnp.log(1.0 + jnp.exp2(jnp.minimum(product, 100.0))), product)
+            scores = lax.dot_general(query[...], kvg[block], NT, preferred_element_type=F32)
+            scores = scores * (LOG2E / math.sqrt(HEAD)) + shift
+            drop = LOG2E * jnp.log(1.0 + jnp.exp2(jnp.minimum(scores, 100.0)))
+            drop = jnp.maximum(drop, scores)
+            takes.append(scores - drop)
             if diagonal:
                 visible = iota((ROWS, ROWS), 1) < iota((ROWS, ROWS), 0)
                 drop = jnp.where(visible, drop, 0.0)
-            scores.append(product)
-            high, low = split_two(drop)
-            at = pl.ds(n * ROWS, ROWS)
-            drops[at, :ROWS] = high
-            drops[at, ROWS:] = low
+            firsts.append(drop[:, :1])
+            drops[pl.ds(n * ROWS, ROWS), :] = drop.astype(BF16)
         passed = jnp.zeros((ROWS, 1), F32)
         sums = jnp.zeros((ROWS, 128), F32)
         totals = dot(drops[pl.ds(0, count * ROWS), :], tri[...])
         for n, block in enumerate(blocks):
             total = totals[n * ROWS : (n + 1) * ROWS]
-            weights = jnp.exp2(scores[n] - (total + passed))
+            weights = jnp.exp2(takes[n] - (total + passed))
             if diagonal:
                 weights = jnp.where(visible, weights, 0.0)
             sums = sums + dot(weights.astype(BF16), kvg[block])
-            passed = passed + total[:, :1]
+            passed = passed + total[:, :1] + firsts[n]
         return sums, passed
 
     def attend_near(blocks):
-        sums, passed = attend(blocks, False)
+        sums, passed = attend(blocks)
         acc[...] += jnp.exp2(-carry[...]) * sums
         carry[...] += passed
 
@@ -314,10 +319,14 @@
         def _():
             attend_near(row_blocks(z - back))
 
-    def far_row(back):
-        @pl.when(z >= back)
+    def help_row(turn):
+        @pl.when(z == turn)
         def _():
-            sums, passed = attend(row_blocks(z - back), False)
+            remote(q_pad, q_help, q_send, q_recv, partner).wait_recv()
+
+        @pl.when(z <= turn)
+        def _():
+            sums, passed = attend(row_blocks(turn - z), query=q_help)
             far[...] = sums + jnp.exp2(-passed) * far[...]
 
     def ring(buffer, pieces, send_sem, recv_sem, hand_sem):
@@ -361,25 +370,54 @@
     grid_start, grid_step, grid_handed, grid_drain = ring(
         grid, GRID_PIECES, grid_send, grid_recv, grid_hand
     )
-    att_start, att_step, att_handed, att_drain = ring(
-        att, ATT_PIECES, att_send, att_recv, att_hand
-    )
-
-    arrived = grid.at[tp, pl.ds(0, SLOTS - CAP)]
-    remote(arrived, arrived, disp_send, disp_recv, partner).wait_recv()
-    grid_start()
-    kv_across()
+
+    def att_copy(distance, device):
+        block = att.at[y_at(distance) * C + c]
+        return remote(block, block, att_send, att_recv.at[y_at(distance)], device)
+
+    def att_hand(distance):
+        block = att.at[y_at(distance) * C + c]
+        remote(block, block, att_send, att_other, partner).start()
+
+    def att_start():
+        for distance in (1, -1, 2, -2):
+            att_copy(0, {"tp_0": y_at(distance)}).start()
+        att_hand(0)
+
+    def att_relay():
+        att_copy(-2, partner).wait_recv()
+        att_copy(-2, {"tp_0": y_at(2)}).start()
+        att_copy(-2, {"tp_0": y_at(1)}).start()
+        att_copy(2, partner).wait_recv()
+        att_copy(2, {"tp_0": y_at(-1)}).start()
+        for distance in (-2, 2):
+            att_hand(distance)
+        for distance in (-1, 1):
+            att_copy(distance, partner).wait_recv()
+            att_hand(distance)
+
+    def att_rest():
+        for distance in (-3, 3, 4):
+            att_copy(distance, partner).wait_recv()
+            att_hand(distance)
+
     loads["offset"].wait()
     sums, passed = attend([ep], True)
     acc[...] = sums
     carry[...] = jnp.broadcast_to(passed, carry.shape)
     far[...] = jnp.zeros(far.shape, F32)
+    kv_step_b(1)
+    kv_across()
     kv_finish(z)
 
     @pl.loop(0, x)
     def _(n):
         attend_near([ep - 1 - n])
 
+    arrived = grid.at[tp, pl.ds(0, SLOTS - CAP)]
+    remote(arrived, arrived, disp_send, disp_recv, partner).wait_recv()
+    grid_start()
+    kv_step_b(2)
     arrived = gains.at[pl.ds(0, N_TP - 1)]
     remote(arrived, arrived, gain_send, gain_recv, partner).wait_recv()
     loads["gate"].wait()
@@ -401,24 +439,27 @@
         for piece in range(GRID_PIECES):
             grid_step(k, piece)
             kv_step(k, piece)
-        kv_step_b(k)
+        if k < 3:
+            kv_step_b(k + 2)
         grid_handed(y_at(1 - k))
         gate_up(y_at(1 - k))
         if k > 1:
             grid_handed(y_at(k - 1))
             gate_up(y_at(k - 1))
-        if k == 2:
+        if k == 1:
             kv_finish(z + Z - 1)
             near_row(1)
+            help_row(0)
+        if k == 2:
+            kv_finish(z + Z - 2)
+            kv_finish(z + 1)
+            near_row(2)
+            help_row(1)
         if k == 3:
-            kv_finish(z + Z - 2)
-            near_row(2)
-            kv_finish(z + 1)
-            far_row(7)
-
-    pieces = wide.at[ep, pl.ds(0, ROWS - 16)]
-    remote(pieces, pieces, wo_send, wo_recv, partner).wait_recv()
-    wide_start()
+            pieces = wide.at[ep, pl.ds(0, ROWS - 16)]
+            remote(pieces, pieces, wo_send, wo_recv, partner).wait_recv()
+            wide_start()
+
     grid_handed(y_at(4))
     gate_up(y_at(4))
     factor = lax.rsqrt(jnp.sum(ssq[...], axis=1, keepdims=True) / D + EPSILON)
@@ -476,15 +517,22 @@
                 way[3][hop, at, :] = total.astype(BF16)
                 sum_copy(way, hop, piece).start()
 
+    wide_across()
+    wide_step_b(1)
     for piece in range(SUM_PIECES):
         sum_step(0, piece)
-    wide_across()
     for distance in (2, -2, 1, -1, 0):
         down(distance)
     kv_finish(z + Z - 3)
+    kv_finish(z + 2)
     near_row(3)
-    kv_finish(z + 2)
-    far_row(6)
+    help_row(2)
+
+    @pl.when(z <= 2)
+    def _():
+        far_out[...] = far[...].astype(BF16)
+        remote(far_out, far_in, far_send, far_recv, across_z).start()
+
 
     def hand_over(row):
         wide_finish(row)
@@ -492,34 +540,37 @@
         at = lax.rem(row, Z)
         remote(wide.at[block], wide_other.at[block], over_send, over_recv.at[at], partner).start()
 
+    wide_step_b(2)
     for piece in range(SUM_PIECES):
         sum_step(1, piece)
         wide_step(1, piece)
-    wide_step_b(1)
+    wide_step_b(3)
     hand_over(z)
+    hand_over(z + Z - 1)
+    hand_over(z + 1)
     kv_finish(z + 3)
-    far_row(5)
     kv_finish(z + Z - 4)
     near_row(4)
-    acc[...] += jnp.exp2(-carry[...]) * far[...]
+
+    @pl.when(z >= 5)
+    def _():
+        remote(far_out, far_in, far_send, far_recv, across_z).wait_recv()
+        acc[...] += jnp.exp2(-carry[...]) * far_in[...].astype(F32)
+
     att[tp] = jnp.transpose(acc[...])[HEAD:].astype(BF16)
     att_start()
     for piece in range(SUM_PIECES):
         sum_step(2, piece)
         wide_step(2, piece)
-    wide_step_b(2)
-    hand_over(z + Z - 1)
-    hand_over(z + 1)
-    for piece in range(ATT_PIECES):
-        att_step(1, piece)
+    wide_step_b(4)
+    hand_over(z + Z - 2)
+    hand_over(z + 2)
+    att_relay()
     for piece in range(SUM_PIECES):
         sum_step(3, piece)
         wide_step(3, piece)
-    wide_step_b(3)
-    hand_over(z + Z - 2)
-    hand_over(z + 2)
-    for piece in range(ATT_PIECES):
-        att_step(2, piece)
+    hand_over(z + Z - 3)
+    hand_over(z + 3)
     wait_pin(y)
     for piece in range(SUM_PIECES):
         at = pl.ds(piece * SUM_ROWS, SUM_ROWS)
@@ -531,7 +582,7 @@
         result[at, :] = total.astype(BF16)
     returned[own_slots, :] = result[own_slots, :]
 
-    @pl.loop(1, N_EP)
+    @pl.loop(1, N_EP, unroll=True)
     def _(distance):
         other, device = ep_peer(distance)
         remote(
@@ -540,18 +591,12 @@
             ret_send, ret_recv, device,
         ).start()
 
+    att_rest()
     for piece in range(X):
         wide_step(4, piece)
-    wide_step_b(4)
-    for piece in range(ATT_PIECES):
-        att_step(3, piece)
-    hand_over(z + Z - 3)
-    hand_over(z + 3)
-    for piece in range(ATT_PIECES):
-        att_step(4, piece)
     hand_over(z + 4)
-    for chip in range(Y):
-        att_handed(chip)
+    blocks = att.at[pl.ds(0, Y)]
+    remote(blocks, blocks, att_send, att_other, partner).wait_recv()
     for row in range(Z):
         block = wide.at[pl.ds(row * X, X)]
         remote(block, block, over_send, over_recv.at[row], partner).wait_recv()
@@ -603,6 +648,15 @@
     exp_copy.start()
 
     kv_drain()
+
+    @pl.when(z >= 5)
+    def _():
+        remote(q_pad, q_help, q_send, q_recv, across_z).wait_send()
+
+    @pl.when(z <= 2)
+    def _():
+        remote(far_out, far_in, far_send, far_recv, across_z).wait_send()
+
     wide_drain()
     remote(wide, wide, over_send, over_recv.at[0], partner).wait_send()
     piece = sent.at[pl.ds(0, SLOTS - CAP)]
@@ -617,7 +671,8 @@
         for piece in (into.at[pl.ds(0, 3)], into.at[3, pl.ds(0, SLOTS // 2)]):
             remote(piece, piece, send_sem, recv_sem.at[0, 0], partner).wait_send()
     grid_drain()
-    att_drain()
+    blocks = att.at[pl.ds(0, N_TP - 1)]
+    remote(blocks, blocks, att_send, att_other, partner).wait_send()
     for copy in (*mix_copies, exp_copy):
         copy.wait()
 
@@ -646,12 +701,15 @@
             pltpu.VMEM((ROWS, D), BF16),
             pltpu.VMEM((4 * HEAD, D), BF16),
             pltpu.VMEM((ROWS, 128), BF16),
+            pltpu.VMEM((ROWS, 128), BF16),
             pltpu.VMEM((N_EP, ROWS, 128), BF16),
             pltpu.VMEM((ROWS, 128), F32),
             pltpu.VMEM((ROWS, 128), F32),
             pltpu.VMEM((ROWS, 128), F32),
-            pltpu.VMEM((X * ROWS, 2 * ROWS), BF16),
-            pltpu.VMEM((2 * ROWS, ROWS), BF16),
+            pltpu.VMEM((ROWS, 128), BF16),
+            pltpu.VMEM((ROWS, 128), BF16),
+            pltpu.VMEM((X * ROWS, ROWS), BF16),
+            pltpu.VMEM((ROWS, ROWS), BF16),
             pltpu.VMEM((SLOTS, TOK), BF16),
             pltpu.VMEM((SLOTS, TOK), BF16),
             pltpu.VMEM((SLOTS, TOK), BF16),
@@ -686,8 +744,9 @@
             dma(()), dma(()), dma(()), dma(()),
             dma(()), dma((Y,)),
             dma(()), dma((4, SUM_PIECES)), dma(()), dma((4, SUM_PIECES)),
-            dma(()), dma((Y, ATT_PIECES)), dma((Y,)),
+            dma(()), dma((Y,)), dma(()),
             dma(()), dma(()),
+            dma(()), dma(()), dma(()), dma(()),
         ],
         compiler_params=pltpu.CompilerParams(
             collective_id=0, has_side_effects=True, vmem_limit_bytes=60 * 1024 * 1024

time: 77.2 us -> 76.4 us (0.990)
  Pallas kernels: 73.5 us -> 72.7 us
    pallas_call x1, Pallas kernels: 73.5 us -> 72.7 us  [on_device(): pl.pallas_call(body, out_shape=(jax.ShapeDtypeStruct((ROWS, D), BF16), ja...]
where the time goes in v4:
time: 76.4 us; the launch traced here: 76.3 us
  Pallas kernels  72.7 us (95%)
  local copies, waits for them, and re-layouts  2.92 us (4%)
    pallas_call x1, Pallas kernels, on_device(): pl.pallas_call(body, out_shape=(jax.ShapeDtypeStruct((ROWS, D), BF16), ja...  72.7 us
    unnamed x4, local copies, waits for them, and re-layouts  2.92 us

profile of v4, /device:TPU:1, one launch (start us, length us, event | category | flops | bytes accessed | tf_op | source)
XLA Modules:
  0.0 76.3 jit_solution(9405232922219351624)
XLA Ops:
  0.6 72.7 %shard_map.158 = (bf16[256,2048]{1,0:T(8,128)(2,1)}, bf16[96,128]{1,0:T(8,128)(2,1)}) custom-call(bf16[256,2048]{1,0:T(8,128)(2,1)} %mix_rows.1, bf16[16,128]{1,0:T(8,128)(2,1)} %bitcast.5, bf16[64,2048]{1,0:T(8,128)(2,1)} %w_query.1, bf16[64,2048]{1,0:T(8,128)(2,1)} %w_key.1, bf16[64,2048]{1,0:T(8,128)(2,1)} %w_value.1, f32[1,8192]{1,0:T(1,128)} %key_offset.1, ...), custom_call_target="tpu_custom_call" | custom-call | tf_op jit(solution)/shard_map/pallas_call | solution.py:685
  73.4 0.0 copy-start
  73.4 2.3 %copy.19 = bf16[256,2048]{1,0:T(8,128)(2,1)} copy(bf16[256,2048]{1,0:T(8,128)(2,1)} %get-tuple-element.4) | data formatting | bytes 2097152
  75.7 0.0 copy-done
  75.7 0.6 copy.20
Async XLA Ops:
  73.4 2.3 %copy-start = (bf16[96,128]{1,0:T(8,128)(2,1)S(1)}, bf16[96,128]{1,0:T(8,128)(2,1)}, u32[]{:S(2)}) copy-start(bf16[96,128]{1,0:T(8,128)(2,1)} %get-tuple-element.5) | copy-start | bytes 73732

commit v5 on v4

--- a/solution.py
+++ b/solution.py
@@ -417,7 +417,6 @@
     arrived = grid.at[tp, pl.ds(0, SLOTS - CAP)]
     remote(arrived, arrived, disp_send, disp_recv, partner).wait_recv()
     grid_start()
-    kv_step_b(2)
     arrived = gains.at[pl.ds(0, N_TP - 1)]
     remote(arrived, arrived, gain_send, gain_recv, partner).wait_recv()
     loads["gate"].wait()
@@ -439,8 +438,8 @@
         for piece in range(GRID_PIECES):
             grid_step(k, piece)
             kv_step(k, piece)
-        if k < 3:
-            kv_step_b(k + 2)
+        if k < 4:
+            kv_step_b(k + 1)
         grid_handed(y_at(1 - k))
         gate_up(y_at(1 - k))
         if k > 1:
@@ -540,37 +539,38 @@
         at = lax.rem(row, Z)
         remote(wide.at[block], wide_other.at[block], over_send, over_recv.at[at], partner).start()
 
-    wide_step_b(2)
     for piece in range(SUM_PIECES):
         sum_step(1, piece)
         wide_step(1, piece)
-    wide_step_b(3)
+    wide_step_b(2)
     hand_over(z)
-    hand_over(z + Z - 1)
-    hand_over(z + 1)
     kv_finish(z + 3)
     kv_finish(z + Z - 4)
     near_row(4)
-
-    @pl.when(z >= 5)
-    def _():
-        remote(far_out, far_in, far_send, far_recv, across_z).wait_recv()
-        acc[...] += jnp.exp2(-carry[...]) * far_in[...].astype(F32)
-
-    att[tp] = jnp.transpose(acc[...])[HEAD:].astype(BF16)
-    att_start()
+    def att_begin():
+        @pl.when(z >= 5)
+        def _():
+            remote(far_out, far_in, far_send, far_recv, across_z).wait_recv()
+            acc[...] += jnp.exp2(-carry[...]) * far_in[...].astype(F32)
+
+        att[tp] = jnp.transpose(acc[...])[HEAD:].astype(BF16)
+        att_start()
+
     for piece in range(SUM_PIECES):
         sum_step(2, piece)
         wide_step(2, piece)
+        if piece == 1:
+            att_begin()
+    wide_step_b(3)
+    hand_over(z + Z - 1)
+    hand_over(z + 1)
+    for piece in range(SUM_PIECES):
+        sum_step(3, piece)
+        wide_step(3, piece)
+    att_relay()
     wide_step_b(4)
     hand_over(z + Z - 2)
     hand_over(z + 2)
-    att_relay()
-    for piece in range(SUM_PIECES):
-        sum_step(3, piece)
-        wide_step(3, piece)
-    hand_over(z + Z - 3)
-    hand_over(z + 3)
     wait_pin(y)
     for piece in range(SUM_PIECES):
         at = pl.ds(piece * SUM_ROWS, SUM_ROWS)
@@ -594,6 +594,8 @@
     att_rest()
     for piece in range(X):
         wide_step(4, piece)
+    hand_over(z + Z - 3)
+    hand_over(z + 3)
     hand_over(z + 4)
     blocks = att.at[pl.ds(0, Y)]
     remote(blocks, blocks, att_send, att_other, partner).wait_recv()

time: 76.4 us -> 72.8 us (0.953)
  Pallas kernels: 72.7 us -> 68.8 us
    pallas_call x1, Pallas kernels: 72.7 us -> 68.8 us  [on_device(): pl.pallas_call(body, out_shape=(jax.ShapeDtypeStruct((ROWS, D), BF16), ja...]
where the time goes in v5:
time: 72.8 us; the launch traced here: 72.4 us
  Pallas kernels  68.8 us (95%)
  local copies, waits for them, and re-layouts  2.92 us (4%)
    pallas_call x1, Pallas kernels, on_device(): pl.pallas_call(body, out_shape=(jax.ShapeDtypeStruct((ROWS, D), BF16), ja...  68.8 us
    unnamed x4, local copies, waits for them, and re-layouts  2.92 us

profile of v5, /device:TPU:1, one launch (start us, length us, event | category | flops | bytes accessed | tf_op | source)
XLA Modules:
  0.0 72.4 jit_solution(7624812065231892925)
XLA Ops:
  0.6 68.8 %shard_map.158 = (bf16[256,2048]{1,0:T(8,128)(2,1)}, bf16[96,128]{1,0:T(8,128)(2,1)}) custom-call(bf16[256,2048]{1,0:T(8,128)(2,1)} %mix_rows.1, bf16[16,128]{1,0:T(8,128)(2,1)} %bitcast.5, bf16[64,2048]{1,0:T(8,128)(2,1)} %w_query.1, bf16[64,2048]{1,0:T(8,128)(2,1)} %w_key.1, bf16[64,2048]{1,0:T(8,128)(2,1)} %w_value.1, f32[1,8192]{1,0:T(1,128)} %key_offset.1, ...), custom_call_target="tpu_custom_call" | custom-call | tf_op jit(solution)/shard_map/pallas_call | solution.py:687
  69.5 0.0 copy-start
  69.5 2.3 %copy.19 = bf16[256,2048]{1,0:T(8,128)(2,1)} copy(bf16[256,2048]{1,0:T(8,128)(2,1)} %get-tuple-element.4) | data formatting | bytes 2097152
  71.8 0.0 copy-done
  71.8 0.6 copy.20
Async XLA Ops:
  69.5 2.3 %copy-start = (bf16[96,128]{1,0:T(8,128)(2,1)S(1)}, bf16[96,128]{1,0:T(8,128)(2,1)}, u32[]{:S(2)}) copy-start(bf16[96,128]{1,0:T(8,128)(2,1)} %get-tuple-element.5) | copy-start | bytes 73732
